TPU v7x, 128 devices: a whole 4x4x4 slice. The times are simulated.
128 devices in a mesh: sp: 64 (over z, y, x), tp: 2 (over core).
Axes of the slice: x: 4, y: 4, z: 4, core: 2. Of those that a mesh axis runs over, the one named last changes fastest.
Arguments:
- stream: bfloat16 [32768, 2048], P(('sp', 'tp')), may hold values from -6 to 6
- queries: bfloat16 [32768, 512], P('sp', 'tp'), may hold values from -6 to 6
- key_rows: bfloat16 [32768, 512], P('sp', 'tp'), may hold values from -6 to 6
- value_rows: bfloat16 [32768, 1024], P('sp', 'tp'), may hold values from -6 to 6
- out_gate: bfloat16 [32768, 1024], P('sp', 'tp'), may hold values from -6 to 6
- in_gate: float32 [4, 32768], P('tp', 'sp'), may hold values from -4 to 214
- forget_gate: float32 [4, 32768], P('tp', 'sp'), may hold values from -2 to 20
- out_proj: bfloat16 [1024, 2048], replicated, may hold values from -0.1875 to 0.1875
- ffn_gain: float32 [2048], replicated, may hold values from 0.1 to 1.9
- gate_proj: bfloat16 [64, 2048, 768], P('sp', None, 'tp'), may hold values from -0.125 to 0.125
- up_proj: bfloat16 [64, 2048, 768], P('sp', None, 'tp'), may hold values from -0.125 to 0.125
- down_proj: bfloat16 [64, 768, 2048], P('sp', 'tp'), may hold values from -0.21875 to 0.21875
- expert_ids: int32 [32768, 2], P(('sp', 'tp')), may hold values from 0 to 63, as said below
- route_weights: float32 [32768, 2], P(('sp', 'tp')), may hold values from 0.05 to 1
Outputs:
- result_stream: bfloat16 [32768, 2048], P(('sp', 'tp'))
Inputs may be any that keep to these rules, and one draw needn't show every extreme that they name: `expert_ids`: both experts of a row are different and lie in one group (expert // 8 equal). In the rows of one device (aligned blocks of 256 rows) each expert is named at most 16 times, some expert exactly 16 times, and each expert shares its rows with a single partner.
All inputs are finite; a program needn't handle non-finite values.
Results may differ from a plain program's by a relative error of at most 0.012.
Values may be sent and summed in bfloat16 or wider, within the bound.
A program may use at most 128 MiB of HBM per device.

v0:
```python
import jax
import jax.numpy as jnp
from jax import lax
from jax.sharding import Mesh
from jax.sharding import PartitionSpec as P

QK = 128
V_DIM = 256
BLOCK = 64
SP = ("sp_0", "sp_1", "sp_2")
SP_TP = ("sp_0", "sp_1", "sp_2", "tp")


epsilon = 1e-06
floor_level = -1e30


def neutral_like(array, identity):
    return jax.tree.map(
        lambda a, e: jnp.broadcast_to(jnp.asarray(e, a.dtype), a.shape), array, identity
    )


def gathered_once(array, axis):
    leaves = jax.tree.leaves(array)
    sequence = sorted(range(len(leaves)), key=lambda k: -leaves[k].size)
    width = (1, *leaves[sequence[0]].shape)[-1]
    lines = [
        jnp.pad(leaves[k].reshape(-1), (0, -leaves[k].size % width)).reshape(-1, width)
        for k in sequence
    ]
    both, at, found = (lax.all_gather(jnp.concatenate(lines), axis), 0, {})
    for k, line in zip(sequence, lines):
        share = both[:, at : at + len(line)].reshape(len(both), -1)
        found[k] = share[:, : leaves[k].size].reshape(-1, *leaves[k].shape)
        at += len(line)
    numbers = iter(range(len(leaves)))
    return jax.tree.map(lambda _: found[next(numbers)], array)


def prefix_by_axis(array, axes, combine, identity):
    before = start = neutral_like(array, identity)
    total = array
    for axis in reversed(axes):
        count, position = (lax.axis_size(axis), lax.axis_index(axis))
        pieces = gathered_once(total, axis)
        inside, total = (start, start)
        for k in range(count):
            passed = k < position
            total = combine(total, jax.tree.map(lambda part: part[k], pieces))
            inside = jax.tree.map(lambda new, old: jnp.where(passed, new, old), total, inside)
        before = combine(inside, before)
    return before


def rows_first(arrays, axis, dims):
    turned = [jnp.moveaxis(a, dim, 0) for a, dim in zip(arrays, dims)]
    both = jnp.concatenate([t.reshape(len(t), -1) for t in turned], axis=1)
    result, at, gathered = (lax.all_gather(both, axis, axis=0, tiled=True), 0, [])
    for t, dim in zip(turned, dims):
        share = result[:, at : at + t[0].size].reshape(-1, *t.shape[1:])
        gathered.append(jnp.moveaxis(share, 0, dim))
        at += t[0].size
    return tuple(gathered)


def join_states(earlier, later):
    early_state, early_level, early_decay = earlier
    late_state, late_level, late_decay = later
    level = jnp.maximum(late_decay + early_level, late_level)
    state = (
        early_state * jnp.exp(late_decay + early_level - level)[:, None, None]
        + late_state * jnp.exp(late_level - level)[:, None, None]
    )
    return (state, level, early_decay + late_decay)


def body(
    stream,
    queries,
    key_rows,
    value_rows,
    out_gate,
    in_gate,
    forget_gate,
    out_proj,
    ffn_gain,
    gate_proj,
    up_proj,
    down_proj,
    expert_ids,
    route_weights,
):
    heads_here, length = in_gate.shape
    blocks = length // BLOCK

    def per_head(rows, size):
        return (
            rows.astype(jnp.float32).reshape(blocks, BLOCK, heads_here, size).transpose(2, 0, 1, 3)
        )

    query_blocks = per_head(queries, QK)
    key_blocks = per_head(key_rows, QK) * QK ** (-0.5)
    value_blocks = per_head(value_rows, V_DIM)
    input_gate = in_gate.reshape(heads_here, blocks, BLOCK)
    cumulative = jnp.cumsum(
        jax.nn.log_sigmoid(forget_gate).reshape(heads_here, blocks, BLOCK), axis=-1
    )
    closing = cumulative[..., -1]
    causal = jnp.tril(jnp.ones((BLOCK, BLOCK), dtype=bool))
    log_inner = jnp.where(
        causal,
        cumulative[..., :, None] - cumulative[..., None, :] + input_gate[..., None, :],
        -jnp.inf,
    )
    log_close = closing[..., None] - cumulative + input_gate

    def advance(carry, inputs):
        state, level, decay = carry
        key_block, value_block, close_block, last_block = inputs
        new_level = jnp.maximum(last_block + level, jnp.max(close_block, axis=-1))
        weight = jnp.exp(close_block - new_level[:, None])
        update = jnp.einsum("hl,hld,hle->hde", weight, key_block, value_block)
        new_state = state * jnp.exp(last_block + level - new_level)[:, None, None] + update
        return ((new_state, new_level, decay + last_block), (state, level, decay))

    empty = (
        jnp.zeros((heads_here, QK, V_DIM), jnp.float32),
        jnp.full((heads_here,), floor_level, jnp.float32),
        jnp.zeros((heads_here,), jnp.float32),
    )
    summary, before = lax.scan(
        advance,
        empty,
        (
            jnp.moveaxis(key_blocks, 1, 0),
            jnp.moveaxis(value_blocks, 1, 0),
            jnp.moveaxis(log_close, 1, 0),
            closing.T,
        ),
    )
    carried = prefix_by_axis(summary, SP, join_states, empty)
    anchor = join_states(
        (
            jnp.zeros((heads_here, QK, V_DIM), jnp.float32),
            jnp.zeros((heads_here,), jnp.float32),
            jnp.zeros((heads_here,), jnp.float32),
        ),
        carried,
    )
    anchor_state, anchor_level, _ = anchor
    block_states, block_levels, block_decays = before
    levels = jnp.maximum(block_decays + anchor_level[None, :], block_levels)
    states = (
        anchor_state[None] * jnp.exp(block_decays + anchor_level[None, :] - levels)[..., None, None]
        + block_states * jnp.exp(block_levels - levels)[..., None, None]
    )
    states = jnp.moveaxis(states, 0, 1)
    levels = levels.T
    log_inter = cumulative + levels[..., None]
    peak = jnp.maximum(log_inter, jnp.max(log_inner, axis=-1))
    scores = jnp.einsum("hntd,hnsd->hnts", query_blocks, key_blocks) * jnp.exp(
        log_inner - peak[..., None]
    )
    from_state = jnp.einsum("hntd,hnde->hnte", query_blocks, states)
    from_block = jnp.einsum("hnts,hnse->hnte", scores, value_blocks)
    numerator = jnp.exp(log_inter - peak)[..., None] * from_state + from_block
    numerator = numerator.transpose(1, 2, 0, 3).reshape(length, heads_here, V_DIM)
    scaled = numerator * lax.rsqrt(
        jnp.mean(numerator * numerator, axis=-1, keepdims=True) + epsilon
    )
    gated = scaled.reshape(length, heads_here * V_DIM) * jax.nn.sigmoid(
        out_gate.astype(jnp.float32)
    )
    heads_out = gated.astype(jnp.bfloat16)
    rows_here, model_width = stream.shape
    token_heads = lax.all_to_all(heads_out, "tp", split_axis=0, concat_axis=1, tiled=True)
    mix = jnp.dot(token_heads, out_proj, preferred_element_type=jnp.float32)
    middle = (stream.astype(jnp.float32) + mix).astype(jnp.bfloat16)
    middle_float = middle.astype(jnp.float32)
    normed = (
        middle_float
        * lax.rsqrt(jnp.mean(middle_float * middle_float, axis=-1, keepdims=True) + epsilon)
        * ffn_gain
    ).astype(jnp.bfloat16)
    experts_total = lax.axis_size(SP)
    per_token = expert_ids.shape[1]
    capacity = 2 * per_token * rows_here // experts_total
    flat_ids = expert_ids.reshape(-1)
    onehot = (flat_ids[:, None] == jnp.arange(experts_total, dtype=jnp.int32)[None, :]).astype(
        jnp.int32
    )
    slot_rank = jnp.sum((jnp.cumsum(onehot, axis=0) - onehot) * onehot, axis=1)
    slot_index = flat_ids * capacity + slot_rank
    owners = (
        jnp.zeros((experts_total * capacity,), jnp.int32)
        .at[slot_index]
        .set(jnp.arange(rows_here * per_token, dtype=jnp.int32) // per_token)
    )
    filled = jnp.zeros((experts_total * capacity,), jnp.bfloat16).at[slot_index].set(1)
    outgoing = (normed[owners] * filled[:, None]).reshape(experts_total, capacity, model_width)
    gate_full, up_full, down_full = rows_first(
        (gate_proj[0], up_proj[0], down_proj[0]), "tp", (1, 1, 0)
    )
    arrived = lax.all_to_all(outgoing, SP, split_axis=0, concat_axis=0, tiled=True)
    sources, amount, _ = arrived.shape
    flattened = arrived.reshape(sources * amount, model_width)
    hidden = (
        jax.nn.silu(jnp.dot(flattened, gate_full, preferred_element_type=jnp.float32))
        * jnp.dot(flattened, up_full, preferred_element_type=jnp.float32)
    ).astype(jnp.bfloat16)
    returned = lax.all_to_all(
        jnp.dot(hidden, down_full, preferred_element_type=jnp.float32)
        .astype(jnp.bfloat16)
        .reshape(sources, amount, model_width),
        SP,
        split_axis=0,
        concat_axis=0,
        tiled=True,
    )
    picked = (
        returned.reshape(experts_total * capacity, model_width)[slot_index]
        .reshape(rows_here, per_token, model_width)
        .astype(jnp.float32)
    )
    expert_sum = jnp.sum(picked * route_weights[..., None], axis=1)
    return (middle_float + expert_sum).astype(jnp.bfloat16)


def solution(mesh):
    split = Mesh(mesh.devices.reshape(4, 4, 4, mesh.shape["tp"]), ("sp_0", "sp_1", "sp_2", "tp"))
    return jax.shard_map(
        body,
        mesh=split,
        in_specs=(
            P(SP_TP, None),
            P(SP, "tp"),
            P(SP, "tp"),
            P(SP, "tp"),
            P(SP, "tp"),
            P("tp", SP),
            P("tp", SP),
            P(),
            P(),
            P(SP, None, "tp"),
            P(SP, None, "tp"),
            P(SP, "tp", None),
            P(SP_TP, None),
            P(SP_TP, None),
        ),
        out_specs=P(SP_TP, None),
        check_vma=False,
    )
```

profile of v0, /device:TPU:0, one launch (start us, length us, event | category | flops | bytes accessed | tf_op | source)
XLA Modules:
  0.0 310.2 jit_solution(12298120856255152876)
XLA Ops:
  7.9 0.8 reshape.1456
  8.9 1.0 convert_multiply_fusion.2
  10.1 1.2 reshape.1457
  11.3 11.7 %while.21 = (s32[]{:T(128)}, f32[2,128,256]{2,1,0:T(8,128)S(1)}, f32[2]{0:T(128)S(1)}, f32[2]{0:T(128)S(1)}, f32[8,2,128,256]{3,2,1,0:T(8,128)}, /*index=5*/f32[...) while((s32[]{:T(128)}, f32[2,128,256]{2,1,0:T(8,128)S(1)}, ...), condition=%wide.region_3.4_spmd.clone, body=%wide.region_1.3_spmd.clone.sunk | while | flops 8667405 | bytes 1445693 | solution.py:132
  11.6 0.7 bitcast_dynamic-update-slice_fusion.2
  13.0 0.7 bitcast_dynamic-update-slice_fusion.2
  14.5 0.7 bitcast_dynamic-update-slice_fusion.2
  16.0 0.8 bitcast_dynamic-update-slice_fusion.2
  17.4 0.7 bitcast_dynamic-update-slice_fusion.2
  18.9 0.7 bitcast_dynamic-update-slice_fusion.2
  20.4 0.7 bitcast_dynamic-update-slice_fusion.2
  21.8 0.7 bitcast_dynamic-update-slice_fusion.2
  23.1 0.7 maximum_bitcast_fusion
  23.9 26.7 %all-gather.13.cloned.1.call-done = f32[4,258,256]{2,1,0:T(8,128)} async-done(((f32[1,258,256]{2,1,0:T(8,128)}), f32[4,258,256]{2,1,0:T(8,128)}) %all-gather.13.cloned.1.call-update) | async-done | bytes 1056784 | tf_op jit(solution)/shard_map/all_gather | solution.py:32
  50.6 0.8 fusion.118
  52.6 1.5 fusion.48
  54.1 0.7 maximum_bitcast_fusion.1
  55.0 24.7 %all-gather.15.cloned.1.call-done = f32[4,258,256]{2,1,0:T(8,128)} async-done(((f32[1,258,256]{2,1,0:T(8,128)}), f32[4,258,256]{2,1,0:T(8,128)}) %all-gather.15.cloned.1.call-update) | async-done | bytes 1056784 | tf_op jit(solution)/shard_map/all_gather | solution.py:32
  79.7 0.8 fusion.117
  82.2 1.5 fusion.41
  84.6 0.8 copy.74
  85.3 1.7 copy.75
  87.1 3.5 %pad_maximum_fusion = bf16[384,6144]{1,0:T(8,128)(2,1)} fusion(bf16[384,2048]{1,0:T(8,128)(2,1)} %bitcast.503, bf16[384,2048]{1,0:T(8,128)(2,1)S(1)} %bitcast.490, bf16[384,2048]{1,0:T(8,128)(2,1)S(1)} %bitcast.489), kind=kLoop, calls=%fused_computation.23 | loop fusion | flops 14155776 | bytes 9437184 | tf_op jit(solution)/shard_map/concatenate | solution.py:58
  92.2 1.2 reduce-window.6
  94.1 2.4 scatter_custom_fusion
  96.6 3.9 %scatter_custom_fusion.1 = bf16[1024]{0:T(1024)(128)(2,1)S(1)} fusion(s32[512]{0:T(512)S(1)} %bitcast.541, bf16[512]{0:T(512)(128)(2,1)S(1)} %broadcast.1063, bf16[]{:T(256)} %constant.103.clone.1), kind=kCustom, calls=%fused_computation.138 | custom fusion | bytes 2050 | tf_op jit(solution)/shard_map/scatter | solution.py:200
  100.6 1.0 fusion.115
  101.6 1.0 fusion.114
  102.7 6.8 %all-gather.17.cloned.1.call-done = f32[4,258,256]{2,1,0:T(8,128)} async-done(((f32[1,258,256]{2,1,0:T(8,128)}), f32[4,258,256]{2,1,0:T(8,128)}) %all-gather.17.cloned.1.call-update) | async-done | bytes 1056784 | tf_op jit(solution)/shard_map/all_gather | solution.py:32
  109.4 0.8 fusion.116
  110.7 1.3 fusion.113
  112.1 2.0 multiply_add_fusion
  114.1 2.1 fusion.28
  116.2 0.8 multiply_reduce_fusion.1
  118.0 0.8 copy.67
  119.5 4.2 %all_to_all.29 = bf16[2,256,512]{1,2,0:T(8,128)(2,1)S(1)} all-to-all(bf16[2,256,512]{1,2,0:T(8,128)(2,1)S(1)} %copy.69), channel_id=1, replica_groups=mesh['sp_0'=4,'sp_1'=4,'sp_2'=4,'tp'=2] {'tp'}, dimensions={0} | all-to-all | bytes 1048576 | tf_op jit(solution)/shard_map/all_to_all | solution.py:177
  123.7 4.4 %fusion.14 = (f32[256]{0:T(256)S(1)}, bf16[256,2048]{1,0:T(8,128)(2,1)S(1)}) fusion(bf16[256,1024]{0,1:T(8,128)(2,1)S(1)} %bitcast.517, bf16[1024,2048]{1,0:T(8,128)(2,1)} %param.23, bf16[256,2048]{1,0:T(8,128)(2,1)S(1)} %copy-done.24), kind=kOutput, calls=%fused_computation.37 | convolution fusion | flops 1076887296 | bytes 6816768 | tf_op jit(solution)/shard_map/dot_general | solution.py:178
  128.4 6.0 %gather_fusion = bf16[1024,2048]{1,0:T(8,128)(2,1)} fusion(bf16[256,2048]{1,0:T(8,128)(2,1)S(1)} %fusion.16, s32[1024]{0:T(1024)S(1)} %fusion.69), kind=kCustom, calls=%fused_computation | custom fusion | bytes 8392704 | tf_op jit(solution)/shard_map/gather | solution.py:201
  134.5 2.5 broadcast_multiply_fusion
  137.0 62.2 %all_to_all.30 = bf16[64,16,2048]{2,1,0:T(8,128)(2,1)} all-to-all(bf16[64,16,2048]{2,1,0:T(8,128)(2,1)S(1)} %broadcast_multiply_fusion), channel_id=1, replica_groups=mesh['sp_0'=4,'sp_1'=4,'sp_2'=4,'tp'=2] {'sp_0','sp_1','sp_2'}, dimensions={0} | all-to-all | bytes 8388608 | tf_op jit(solution)/shard_map/all_to_all | solution.py:205
  199.3 8.3 %fusion.9 = f32[1024,768]{1,0:T(8,128)} fusion(bf16[1024,2048]{1,0:T(8,128)(2,1)} %bitcast.495, bf16[768,6144]{1,0:T(8,128)(2,1)} %all-gather.11.cloned.1.call-done), kind=kOutput, calls=%fused_computation.27 | convolution fusion | flops 3221225472 | bytes 10485760 | tf_op jit(solution)/shard_map/dot_general | solution.py:210
  207.5 13.6 %convolution_convert_fusion = bf16[1024,2048]{1,0:T(8,128)(2,1)} fusion(bf16[768,6144]{1,0:T(8,128)(2,1)} %all-gather.11.cloned.1.call-done, f32[1024,768]{1,0:T(8,128)} %fusion.9, bf16[1024,2048]{1,0:T(8,128)(2,1)} %bitcast.496), kind=kOutput, calls=%fused_computation.25 | convolution fusion | flops 6449266688 | bytes 17825792 | tf_op jit(solution)/shard_map/dot_general | solution.py:213
  221.2 6.3 %all-to-all-start.2 = ((bf16[64,16,2048]{2,1,0:T(8,128)(2,1)}), bf16[64,16,2048]{2,1,0:T(8,128)(2,1)}, u32[]{:S(2)}, u32[]{:S(2)}) async-start(bf16[64,16,2048]{2,1,0:T(8,128)(2,1)} %bitcast.494), calls=%async_computation.2 | async-start | bytes 8388608 | tf_op jit(solution)/shard_map/all_to_all | solution.py:212
  227.7 54.7 %all-to-all-done.2 = bf16[64,16,2048]{2,1,0:T(8,128)(2,1)} async-done(((bf16[64,16,2048]{2,1,0:T(8,128)(2,1)}), bf16[64,16,2048]{2,1,0:T(8,128)(2,1)}, u32[]{:S(2)}, u32[]{:S(2)}) %all-to-all-start.2) | async-done | bytes 4194336 | tf_op jit(solution)/shard_map/all_to_all | solution.py:212
  282.4 7.1 %gather_fusion.1 = bf16[512,2048]{1,0:T(8,128)(2,1)S(1)} fusion(bf16[1024,2048]{1,0:T(8,128)(2,1)} %bitcast.105, s32[1024]{0:T(1024)S(1)} %pad_clamp_fusion), kind=kCustom, calls=%fused_computation.1 | custom fusion | bytes 4196352 | tf_op jit(solution)/shard_map/gather | solution.py:222
  289.5 4.0 %reshape.1477 = f32[256,2,2048]{2,1,0:T(2,128)} reshape(bf16[512,2048]{1,0:T(8,128)(2,1)S(1)} %gather_fusion.1) | data formatting | bytes 6291456 | tf_op jit(solution)/shard_map/convert_element_type | solution.py:224
  293.5 8.9 %multiply_reduce_fusion = f32[256,2048]{1,0:T(8,128)S(1)} fusion(f32[256,2,2048]{2,1,0:T(2,128)} %reshape.1477, f32[256,2]{1,0:T(8,128)S(1)} %copy.76), kind=kLoop, calls=%fused_computation.24 | loop fusion | flops 1572864 | bytes 6293504 | tf_op jit(solution)/shard_map/reduce_sum | solution.py:226
  302.4 1.3 fusion.17
  (230 shorter events, 15.6 us)
Async XLA Ops:
  6.5 44.1 %all-gather.13.cloned.1.call-start = ((), (), s32[]{:S(2)}) async-start(), calls=%async_computation.4 | async-start | bytes 1351680 | tf_op jit(solution)/shard_map/all_gather | solution.py:32
  23.0 61.4 %copy-start.2 = (bf16[8,2,64,256]{3,1,2,0:T(2,128)(2,1)}, bf16[8,2,64,256]{3,1,2,0:T(2,128)(2,1)S(1)}, u32[]{:S(2)}) copy-start(bf16[8,2,64,256]{3,1,2,0:T(2,128)(2,1)S(1)} %get-tuple-element.382) | copy-start | bytes 1572868
  23.1 61.4 %copy-start.4 = (f32[8,2,64,128]{3,1,2,0:T(2,128)}, f32[8,2,64,128]{3,1,2,0:T(2,128)S(1)}, u32[]{:S(2)}) copy-start(f32[8,2,64,128]{3,1,2,0:T(2,128)S(1)} %get-tuple-element.383) | copy-start | bytes 1572868
  23.1 61.5 %copy-start.6 = (bf16[1,2048,384]{2,1,0:T(8,128)(2,1)S(1)}, bf16[1,2048,384]{2,1,0:T(8,128)(2,1)}, u32[]{:S(2)}) copy-start(bf16[1,2048,384]{2,1,0:T(8,128)(2,1)} %param.25) | copy-start | bytes 4718596
  23.9 55.8 %all-gather.15.cloned.1.call-start = ((), (), s32[]{:S(2)}) async-start(), calls=%async_computation.5 | async-start | bytes 1351680 | tf_op jit(solution)/shard_map/all_gather | solution.py:32
  51.5 1.1 copy-start.17
  51.6 3.4 %copy-start.19 = (f32[2]{0:T(128)}, f32[2]{0:T(128)S(1)}, u32[]{:S(2)}) copy-start(f32[2]{0:T(128)S(1)} %get-tuple-element.233) | copy-start | bytes 28
  51.6 28.9 %copy-start.18 = (f32[2]{0:T(128)}, f32[2]{0:T(128)S(1)}, u32[]{:S(2)}) copy-start(f32[2]{0:T(128)S(1)} %get-tuple-element.194) | copy-start | bytes 28
  51.6 0.5 copy-start.22
  54.9 54.5 %all-gather.17.cloned.1.call-start = ((), (), s32[]{:S(2)}) async-start(), calls=%async_computation.6 | async-start | bytes 1351680 | tf_op jit(solution)/shard_map/all_gather | solution.py:32
  81.2 1.0 copy-start.16
  81.2 0.5 copy-start.23
  84.5 114.7 %all-gather.11.cloned.1.call-start = ((), (), s32[]{:S(2)}) async-start(), calls=%async_computation.3 | async-start | bytes 14155776 | tf_op jit(solution)/shard_map/all_gather | solution.py:59
  90.6 0.7 copy-start.14
  90.6 1.5 copy-start.12
  90.6 10.0 %copy-start = (f32[4,258,256]{2,1,0:T(8,128)S(1)}, f32[4,258,256]{2,1,0:T(8,128)}, u32[]{:S(2)}) copy-start(f32[4,258,256]{2,1,0:T(8,128)} %all-gather.13.cloned.1.call-done) | copy-start | bytes 3170308
  90.6 11.0 %copy-start.1 = (f32[4,258,256]{2,1,0:T(8,128)S(1)}, f32[4,258,256]{2,1,0:T(8,128)}, u32[]{:S(2)}) copy-start(f32[4,258,256]{2,1,0:T(8,128)} %all-gather.15.cloned.1.call-done) | copy-start | bytes 3170308
  90.6 19.9 %copy-start.20 = (f32[2]{0:T(128)S(1)}, f32[2]{0:T(128)}, u32[]{:S(2)}) copy-start(f32[2]{0:T(128)} %get-tuple-element.235) | copy-start | bytes 28
  90.6 19.9 %copy-start.21 = (f32[2]{0:T(128)S(1)}, f32[2]{0:T(128)}, u32[]{:S(2)}) copy-start(f32[2]{0:T(128)} %get-tuple-element.236) | copy-start | bytes 28
  101.6 10.4 %copy-start.7 = (f32[1,256,256]{2,1,0:T(8,128)S(1)}, f32[1,256,256]{2,1,0:T(8,128)}, u32[]{:S(2)}) copy-start(f32[1,256,256]{2,1,0:T(8,128)} %get-tuple-element.208) | copy-start | bytes 786436
  101.6 10.4 %copy-start.8 = (f32[1,256,256]{2,1,0:T(8,128)S(1)}, f32[1,256,256]{2,1,0:T(8,128)}, u32[]{:S(2)}) copy-start(f32[1,256,256]{2,1,0:T(8,128)} %get-tuple-element.209) | copy-start | bytes 786436
  101.6 10.4 %copy-start.9 = (f32[1,256,256]{2,1,0:T(8,128)S(1)}, f32[1,256,256]{2,1,0:T(8,128)}, u32[]{:S(2)}) copy-start(f32[1,256,256]{2,1,0:T(8,128)} %get-tuple-element.210) | copy-start | bytes 786436
  101.6 10.4 %copy-start.10 = (f32[1,256,256]{2,1,0:T(8,128)S(1)}, f32[1,256,256]{2,1,0:T(8,128)}, u32[]{:S(2)}) copy-start(f32[1,256,256]{2,1,0:T(8,128)} %get-tuple-element.211) | copy-start | bytes 786436
  112.1 4.2 %copy-start.3 = (bf16[8,2,64,256]{3,1,2,0:T(2,128)(2,1)S(1)}, bf16[8,2,64,256]{3,1,2,0:T(2,128)(2,1)}, u32[]{:S(2)}) copy-start(bf16[8,2,64,256]{3,1,2,0:T(2,128)(2,1)} %copy-done.2) | copy-start | bytes 1572868
  112.1 4.2 %copy-start.5 = (f32[8,2,64,128]{3,1,2,0:T(2,128)S(1)}, f32[8,2,64,128]{3,1,2,0:T(2,128)}, u32[]{:S(2)}) copy-start(f32[8,2,64,128]{3,1,2,0:T(2,128)} %copy-done.4) | copy-start | bytes 1572868
  117.9 1.0 copy-start.11
  118.9 4.8 %copy-start.24 = (bf16[256,2048]{1,0:T(8,128)(2,1)S(1)}, bf16[256,2048]{1,0:T(8,128)(2,1)}, u32[]{:S(2)}) copy-start(bf16[256,2048]{1,0:T(8,128)(2,1)} %param.16) | copy-start | bytes 3145732
  123.7 4.4 %copy-start.13 = (f32[2048]{0:T(1024)S(1)}, f32[2048]{0:T(1024)}, u32[]{:S(2)}) copy-start(f32[2048]{0:T(1024)} %param.24) | copy-start | bytes 24580
  221.2 6.4 %copy-start.15 = (f32[256,2]{0,1:T(2,128)S(1)}, f32[256,2]{0,1:T(2,128)}, u32[]{:S(2)}) copy-start(f32[256,2]{0,1:T(2,128)} %param.29) | copy-start | bytes 6148
  221.2 61.2 %all-to-all-start.2 = ((bf16[64,16,2048]{2,1,0:T(8,128)(2,1)}), bf16[64,16,2048]{2,1,0:T(8,128)(2,1)}, u32[]{:S(2)}, u32[]{:S(2)}) async-start(bf16[64,16,2048]{2,1,0:T(8,128)(2,1)} %bitcast.494), calls=%async_computation.2 | async-start | bytes 8388608 | tf_op jit(solution)/shard_map/all_to_all | solution.py:212
Sparse Core Ops, SparseCore 0:
  24.0 26.6 all-gather.12
  55.0 24.5 all-gather.14
  84.6 24.7 all-gather.16
  110.9 24.5 all-gather.10
where the time goes:
time: 311 us; the launch traced here: 310 us
  waiting for transfers between devices  113 us (36%)
  blocking collectives  66.4 us (21%)
  local copies, waits for them, and re-layouts  41.5 us (13%)
  other arithmetic  36.8 us (12%)
  matrix products  31.8 us (10%)
  between operations  13.9 us (4%)
  starting transfers between devices  6.48 us (2%)
    all_to_all x1, blocking collectives, body(): lax.all_to_all(outgoing, SP, split_axis=0, concat_axis=0, tiled=True)  62.2 us
    all_gather x3, waiting for transfers between devices, gathered_once(): both, at, found = (lax.all_gather(jnp.concatenate(lines), axis), 0, {})  58.2 us
    all_to_all x1, waiting for transfers between devices, body(): lax.all_to_all(jnp.dot(hidden, down_full, preferred_element_type=jnp.floa...  54.7 us
    dot_general x1, matrix products, body(): jnp.dot(hidden, down_full, preferred_element_type=jnp.float32)  13.6 us
    reduce_sum x1, other arithmetic, body(): expert_sum = jnp.sum(picked * route_weights[..., None], axis=1)  8.89 us
    dot_general x1, matrix products, body(): jnp.dot(flattened, up_full, preferred_element_type=jnp.float32)  8.29 us
    gather x1, local copies, waits for them, and re-layouts, body(): returned.reshape(experts_total * capacity, model_width)[slot_index]  7.13 us
    all_to_all x1, starting transfers between devices, body(): lax.all_to_all(jnp.dot(hidden, down_full, preferred_element_type=jnp.floa...  6.35 us
  transfers between devices with their start and end apart: 5, of which 4 were waited for; matrix products, arithmetic and copies ran while one was open for 13% of the time, Pallas kernels for 0%

commit v1 on v0

--- a/solution.py
+++ b/solution.py
@@ -1,9 +1,12 @@
 import jax
 import jax.numpy as jnp
 from jax import lax
+from jax.experimental import pallas as pl
+from jax.experimental.pallas import tpu as pltpu
 from jax.sharding import Mesh
 from jax.sharding import PartitionSpec as P
 
+MESH = pl.DeviceIdType.MESH
 QK = 128
 V_DIM = 256
 BLOCK = 64
@@ -53,17 +56,6 @@
     return before
 
 
-def rows_first(arrays, axis, dims):
-    turned = [jnp.moveaxis(a, dim, 0) for a, dim in zip(arrays, dims)]
-    both = jnp.concatenate([t.reshape(len(t), -1) for t in turned], axis=1)
-    result, at, gathered = (lax.all_gather(both, axis, axis=0, tiled=True), 0, [])
-    for t, dim in zip(turned, dims):
-        share = result[:, at : at + t[0].size].reshape(-1, *t.shape[1:])
-        gathered.append(jnp.moveaxis(share, 0, dim))
-        at += t[0].size
-    return tuple(gathered)
-
-
 def join_states(earlier, later):
     early_state, early_level, early_decay = earlier
     late_state, late_level, late_decay = later
@@ -73,6 +65,239 @@
         + late_state * jnp.exp(late_level - level)[:, None, None]
     )
     return (state, level, early_decay + late_decay)
+
+
+OFFSETS = sorted(
+    ((a, b, c) for a in range(4) for b in range(4) for c in range(4)),
+    key=lambda o: sum(min(v, 4 - v) for v in o),
+)
+SLOT = 16
+GROUP_ROWS = 256
+PER_GROUP = GROUP_ROWS // SLOT
+
+
+def place():
+    return [lax.axis_index(axis) for axis in SP_TP]
+
+
+def peer(here, offset, sign=1):
+    z, y, x, core = here
+    return tuple(lax.rem(p + (sign * o) % 4, 4) for p, o in zip((z, y, x), offset)) + (core,)
+
+
+def experts_kernel(
+    select_ref,
+    weigh_ref,
+    normed_ref,
+    middle_ref,
+    gate_ref,
+    up_ref,
+    down_ref,
+    out_ref,
+    outgoing,
+    arrived,
+    answers,
+    returned,
+    gate_full,
+    up_full,
+    down_full,
+    hidden,
+    total,
+    local_sem,
+    weight_send,
+    weight_recv,
+    send_sem,
+    recv_sem,
+    back_send,
+    back_recv,
+):
+    here = place()
+    other = (here[0], here[1], here[2], 1 - here[3])
+    barrier = pltpu.get_barrier_semaphore()
+    for offset in OFFSETS[1:]:
+        pl.semaphore_signal(barrier, inc=1, device_id=peer(here, offset), device_id_type=MESH)
+    pl.semaphore_signal(barrier, inc=1, device_id=other, device_id_type=MESH)
+    half = gate_ref.shape[1]
+    locals_ = [
+        pltpu.make_async_copy(gate_ref, gate_full.at[:, pl.ds(0, half)], local_sem.at[0]),
+        pltpu.make_async_copy(up_ref, up_full.at[:, pl.ds(0, half)], local_sem.at[1]),
+        pltpu.make_async_copy(down_ref, down_full.at[pl.ds(0, half)], local_sem.at[2]),
+    ]
+    for copy in locals_:
+        copy.start()
+
+    def rows(i):
+        return pl.ds(i * SLOT, SLOT)
+
+    def group(g):
+        return pl.ds(g * GROUP_ROWS, GROUP_ROWS)
+
+    groups = len(OFFSETS) // PER_GROUP
+    tile = 256
+
+    def build(g):
+        pick = select_ref[group(g), :]
+        for n in range(0, outgoing.shape[1], tile):
+            cols = slice(n, n + tile)
+            outgoing[group(g), cols] = jnp.dot(
+                pick, normed_ref[:, cols], preferred_element_type=jnp.float32
+            ).astype(jnp.bfloat16)
+
+    def send(g):
+        for i in range(max(g * PER_GROUP, 1), (g + 1) * PER_GROUP):
+            pltpu.make_async_remote_copy(
+                src_ref=outgoing.at[rows(i)],
+                dst_ref=arrived.at[rows(i)],
+                send_sem=send_sem,
+                recv_sem=recv_sem.at[g],
+                device_id=peer(here, OFFSETS[i]),
+                device_id_type=MESH,
+            ).start()
+
+    build(0)
+    pl.semaphore_wait(barrier, len(OFFSETS))
+    weights = [
+        pltpu.make_async_remote_copy(
+            src_ref=mine,
+            dst_ref=theirs,
+            send_sem=weight_send.at[i],
+            recv_sem=weight_recv.at[i],
+            device_id=other,
+            device_id_type=MESH,
+        )
+        for i, (mine, theirs) in enumerate(
+            (
+                (gate_ref, gate_full.at[:, pl.ds(half, half)]),
+                (up_ref, up_full.at[:, pl.ds(half, half)]),
+                (down_ref, down_full.at[pl.ds(half, half)]),
+            )
+        )
+    ]
+    for g in range(1, groups):
+        build(g)
+        send(g - 1)
+        if g == 1:
+            for copy in weights:
+                copy.start()
+    arrived[rows(0), :] = outgoing[rows(0), :]
+    send(groups - 1)
+
+    def landed(ref, sem, first, last):
+        span = pl.ds(first * SLOT, (last - first) * SLOT)
+        pltpu.make_async_copy(ref.at[span], ref.at[span], sem).wait()
+
+    for copy in locals_:
+        copy.wait()
+    for copy in weights:
+        copy.wait_recv()
+    for g in range(groups):
+        landed(arrived, recv_sem.at[g], max(g * PER_GROUP, 1), (g + 1) * PER_GROUP)
+        block = arrived[group(g), :]
+        for n in range(0, hidden.shape[1], tile):
+            cols = slice(n, n + tile)
+            gates = jnp.dot(block, gate_full[:, cols], preferred_element_type=jnp.float32)
+            ups = jnp.dot(block, up_full[:, cols], preferred_element_type=jnp.float32)
+            hidden[:, cols] = (gates * jax.nn.sigmoid(gates) * ups).astype(jnp.bfloat16)
+        for n in range(0, answers.shape[1], tile):
+            cols = slice(n, n + tile)
+            answers[group(g), cols] = jnp.dot(
+                hidden[...], down_full[:, cols], preferred_element_type=jnp.float32
+            ).astype(jnp.bfloat16)
+        for i in range(max(g * PER_GROUP, 1), (g + 1) * PER_GROUP):
+            pltpu.make_async_remote_copy(
+                src_ref=answers.at[rows(i)],
+                dst_ref=returned.at[rows(i)],
+                send_sem=back_send,
+                recv_sem=back_recv.at[g],
+                device_id=peer(here, OFFSETS[i], -1),
+                device_id_type=MESH,
+            ).start()
+    returned[rows(0), :] = answers[rows(0), :]
+    for g in range(groups):
+        landed(returned, back_recv.at[g], max(g * PER_GROUP, 1), (g + 1) * PER_GROUP)
+        for n in range(0, out_ref.shape[1], tile):
+            cols = slice(n, n + tile)
+            part = jnp.dot(
+                weigh_ref[0, :, group(g)],
+                returned[group(g), cols],
+                preferred_element_type=jnp.float32,
+            ) + jnp.dot(
+                weigh_ref[1, :, group(g)],
+                returned[group(g), cols],
+                preferred_element_type=jnp.float32,
+            )
+            before = middle_ref[:, cols].astype(jnp.float32) if g == 0 else total[:, cols]
+            if g < groups - 1:
+                total[:, cols] = before + part
+            else:
+                out_ref[:, cols] = (before + part).astype(jnp.bfloat16)
+    landed(outgoing, send_sem, 1, len(OFFSETS))
+    landed(answers, back_send, 1, len(OFFSETS))
+    for copy in weights:
+        copy.wait_send()
+
+
+def experts(select, weigh, normed, middle, gate, up, down):
+    rows_here, width = normed.shape
+    slots = select.shape[0]
+    half = gate.shape[1]
+    vmem = pl.BlockSpec(memory_space=pltpu.VMEM)
+    hbm = pl.BlockSpec(memory_space=pl.ANY)
+    dma = pltpu.SemaphoreType.DMA
+    groups = slots // GROUP_ROWS
+    return pl.pallas_call(
+        experts_kernel,
+        out_shape=jax.ShapeDtypeStruct((rows_here, width), jnp.bfloat16),
+        in_specs=[vmem] * 4 + [hbm] * 3,
+        out_specs=vmem,
+        scratch_shapes=[pltpu.VMEM((slots, width), jnp.bfloat16)] * 4
+        + [
+            pltpu.VMEM((width, 2 * half), jnp.bfloat16),
+            pltpu.VMEM((width, 2 * half), jnp.bfloat16),
+            pltpu.VMEM((2 * half, width), jnp.bfloat16),
+            pltpu.VMEM((GROUP_ROWS, 2 * half), jnp.bfloat16),
+            pltpu.VMEM((rows_here, width), jnp.float32),
+            dma((3,)),
+            dma((3,)),
+            dma((3,)),
+            dma(()),
+            dma((groups,)),
+            dma(()),
+            dma((groups,)),
+        ],
+        compiler_params=pltpu.CompilerParams(
+            collective_id=1, has_side_effects=True, vmem_limit_bytes=56 << 20
+        ),
+    )(select, weigh, normed, middle, gate, up, down)
+
+
+def routing(expert_ids, route_weights):
+    rows_here = expert_ids.shape[0]
+    z, y, x, _ = place()
+    table = jnp.array(OFFSETS, jnp.int32)
+    owner = (
+        lax.rem(z + table[:, 0], 4) * 16 + lax.rem(y + table[:, 1], 4) * 4 + lax.rem(x + table[:, 2], 4)
+    )
+    target = (owner[:, None] * SLOT + jnp.arange(SLOT, dtype=jnp.int32)[None, :]).reshape(-1)
+    every = jnp.arange(len(OFFSETS), dtype=jnp.int32)[None, :]
+    named = [expert_ids[:, j : j + 1] == every for j in range(expert_ids.shape[1])]
+    used = jnp.where(named[0] | named[1], 1.0, 0.0).astype(jnp.bfloat16)
+    earlier = jnp.tril(jnp.ones((rows_here, rows_here), jnp.bfloat16), -1)
+    rank = jnp.dot(earlier, used, preferred_element_type=jnp.float32)
+    slots = [
+        expert_ids[:, j] * SLOT + jnp.sum(jnp.where(named[j], rank, 0.0), axis=1).astype(jnp.int32)
+        for j in range(expert_ids.shape[1])
+    ]
+    select = ((target[:, None] == slots[0][None, :]) | (target[:, None] == slots[1][None, :])).astype(
+        jnp.bfloat16
+    )
+    weigh = sum(
+        jnp.where(slots[j][:, None] == target[None, :], route_weights[:, j : j + 1], 0.0)
+        for j in range(2)
+    )
+    high = weigh.astype(jnp.bfloat16)
+    low = (weigh - high.astype(jnp.float32)).astype(jnp.bfloat16)
+    return select, jnp.stack([high, low])
 
 
 def body(
@@ -183,48 +408,8 @@
         * lax.rsqrt(jnp.mean(middle_float * middle_float, axis=-1, keepdims=True) + epsilon)
         * ffn_gain
     ).astype(jnp.bfloat16)
-    experts_total = lax.axis_size(SP)
-    per_token = expert_ids.shape[1]
-    capacity = 2 * per_token * rows_here // experts_total
-    flat_ids = expert_ids.reshape(-1)
-    onehot = (flat_ids[:, None] == jnp.arange(experts_total, dtype=jnp.int32)[None, :]).astype(
-        jnp.int32
-    )
-    slot_rank = jnp.sum((jnp.cumsum(onehot, axis=0) - onehot) * onehot, axis=1)
-    slot_index = flat_ids * capacity + slot_rank
-    owners = (
-        jnp.zeros((experts_total * capacity,), jnp.int32)
-        .at[slot_index]
-        .set(jnp.arange(rows_here * per_token, dtype=jnp.int32) // per_token)
-    )
-    filled = jnp.zeros((experts_total * capacity,), jnp.bfloat16).at[slot_index].set(1)
-    outgoing = (normed[owners] * filled[:, None]).reshape(experts_total, capacity, model_width)
-    gate_full, up_full, down_full = rows_first(
-        (gate_proj[0], up_proj[0], down_proj[0]), "tp", (1, 1, 0)
-    )
-    arrived = lax.all_to_all(outgoing, SP, split_axis=0, concat_axis=0, tiled=True)
-    sources, amount, _ = arrived.shape
-    flattened = arrived.reshape(sources * amount, model_width)
-    hidden = (
-        jax.nn.silu(jnp.dot(flattened, gate_full, preferred_element_type=jnp.float32))
-        * jnp.dot(flattened, up_full, preferred_element_type=jnp.float32)
-    ).astype(jnp.bfloat16)
-    returned = lax.all_to_all(
-        jnp.dot(hidden, down_full, preferred_element_type=jnp.float32)
-        .astype(jnp.bfloat16)
-        .reshape(sources, amount, model_width),
-        SP,
-        split_axis=0,
-        concat_axis=0,
-        tiled=True,
-    )
-    picked = (
-        returned.reshape(experts_total * capacity, model_width)[slot_index]
-        .reshape(rows_here, per_token, model_width)
-        .astype(jnp.float32)
-    )
-    expert_sum = jnp.sum(picked * route_weights[..., None], axis=1)
-    return (middle_float + expert_sum).astype(jnp.bfloat16)
+    select, weigh = routing(expert_ids, route_weights)
+    return experts(select, weigh, normed, middle, gate_proj[0], up_proj[0], down_proj[0])
 
 
 def solution(mesh):

time: 311 us -> 258 us (0.83)
  Pallas kernels: 0 us -> 121 us
  blocking collectives: 66.4 us -> 4.15 us
  waiting for transfers between devices: 113 us -> 71.9 us
  local copies, waits for them, and re-layouts: 41.5 us -> 14.2 us
  matrix products: 31.8 us -> 7.81 us
  other arithmetic: 36.8 us -> 22.3 us
  starting transfers between devices: 6.48 us -> 0.09 us
    pallas_call x0 -> x1, Pallas kernels: none -> 121 us  [experts(): pl.pallas_call(experts_kernel, out_shape=jax.ShapeDtypeStruct((rows_here,...]
    all_to_all x1 -> x0, blocking collectives: 62.2 us -> none  [body(): lax.all_to_all(outgoing, SP, split_axis=0, concat_axis=0, tiled=True)]
    all_to_all x1 -> x0, waiting for transfers between devices: 54.7 us -> none  [body(): lax.all_to_all(jnp.dot(hidden, down_full, preferred_element_type=jnp.floa...]
    dot_general x2 -> x1, matrix products: 21.9 us -> 0.28 us  [routing(): rank = jnp.dot(earlier, used, preferred_element_type=jnp.float32)]
    all_gather x3, waiting for transfers between devices: 58.2 us -> 71.9 us  [gathered_once(): both, at, found = (lax.all_gather(jnp.concatenate(lines), axis), 0, {})]
    gather x2 -> x0, local copies, waits for them, and re-layouts: 13.2 us -> none  [the longest x1 7.13 us: body(): returned.reshape(experts_total * capacity, model_width)[slot_index]]
    reduce_sum x2 -> x0, other arithmetic: 9.01 us -> none  [the longest x1 8.89 us: body(): expert_sum = jnp.sum(picked * route_weights[..., None], axis=1)]
    scatter x2 -> x0, local copies, waits for them, and re-layouts: 6.39 us -> none  [the longest x1 3.95 us: body(): jnp.zeros((experts_total * capacity,), jnp.bfloat16).at[slot_index].set(1)]
  transfers between devices with their start and end apart: 5 -> 3, of which waited for: 4 -> 3; matrix products, arithmetic and copies ran while one was open for 13% -> 2% of each run, Pallas kernels for 0% -> 0%
where the time goes in v1:
time: 258 us; the launch traced here: 256 us
  Pallas kernels  121 us (47%)
  waiting for transfers between devices  71.9 us (28%)
  other arithmetic  22.3 us (9%)
  local copies, waits for them, and re-layouts  14.2 us (6%)
  between operations  13.9 us (5%)
  matrix products  7.81 us (3%)
  blocking collectives  4.15 us (2%)
    pallas_call x1, Pallas kernels, experts(): pl.pallas_call(experts_kernel, out_shape=jax.ShapeDtypeStruct((rows_here,...  121 us
    all_gather x3, waiting for transfers between devices, gathered_once(): both, at, found = (lax.all_gather(jnp.concatenate(lines), axis), 0, {})  71.9 us
    dynamic_update_slice x8, other arithmetic, body(): lax.scan(advance, empty, (jnp.moveaxis(key_blocks, 1, 0), jnp.moveaxis(va...  5.92 us
  transfers between devices with their start and end apart: 3, of which 3 were waited for; matrix products, arithmetic and copies ran while one was open for 2% of the time, Pallas kernels for 0%

profile of v1, /device:TPU:0, one launch (start us, length us, event | category | flops | bytes accessed | tf_op | source)
XLA Modules:
  0.0 256.2 jit_solution(6818404588119877346)
XLA Ops:
  6.6 0.8 fusion.67
  7.4 0.4 reduce_window_sum.13
  8.0 0.8 reshape.1786
  8.9 1.0 convert_multiply_fusion.2
  10.3 11.7 %while.21 = (s32[]{:T(128)}, f32[2,128,256]{2,1,0:T(8,128)S(1)}, f32[2]{0:T(128)S(1)}, f32[2]{0:T(128)S(1)}, f32[8,2,128,256]{3,2,1,0:T(8,128)}, /*index=5*/f32[...) while((s32[]{:T(128)}, f32[2,128,256]{2,1,0:T(8,128)S(1)}, ...), condition=%wide.region_5.6_spmd.clone, body=%wide.region_3.5_spmd.clone.sunk | while | flops 8667405 | bytes 1445693 | solution.py:357
  10.6 0.7 bitcast_dynamic-update-slice_fusion.2
  11.4 0.3 convolution_add_fusion.3
  12.1 0.7 bitcast_dynamic-update-slice_fusion.2
  12.9 0.3 convolution_add_fusion.3
  13.5 0.7 bitcast_dynamic-update-slice_fusion.2
  15.0 0.7 bitcast_dynamic-update-slice_fusion.2
  16.5 0.7 bitcast_dynamic-update-slice_fusion.2
  17.3 0.3 convolution_add_fusion.3
  17.9 0.8 bitcast_dynamic-update-slice_fusion.2
  18.8 0.3 convolution_add_fusion.3
  19.4 0.7 bitcast_dynamic-update-slice_fusion.2
  20.2 0.3 convolution_add_fusion.3
  20.9 0.7 bitcast_dynamic-update-slice_fusion.2
  22.2 0.7 maximum_bitcast_fusion
  23.0 26.7 %all-gather.10.cloned.1.call-done = f32[4,258,256]{2,1,0:T(8,128)} async-done(((f32[1,258,256]{2,1,0:T(8,128)}), f32[4,258,256]{2,1,0:T(8,128)}) %all-gather.10.cloned.1.call-update) | async-done | bytes 1056784 | tf_op jit(solution)/shard_map/all_gather | solution.py:35
  49.7 0.8 fusion.120
  50.8 0.4 copy-done.26
  51.7 1.5 fusion.39
  53.3 0.7 maximum_bitcast_fusion.1
  54.7 0.3 fusion.28
  55.1 23.7 %all-gather.12.cloned.1.call-done = f32[4,258,256]{2,1,0:T(8,128)} async-done(((f32[1,258,256]{2,1,0:T(8,128)}), f32[4,258,256]{2,1,0:T(8,128)}) %all-gather.12.cloned.1.call-update) | async-done | bytes 1056784 | tf_op jit(solution)/shard_map/all_gather | solution.py:35
  78.8 0.8 fusion.119
  79.6 0.6 exponential_multiply_fusion.2
  80.4 0.5 copy-done.27
  81.4 1.5 fusion.32
  82.9 0.7 maximum_bitcast_fusion.2
  84.0 1.1 pad_maximum_fusion.weigh_ref
  85.1 1.0 or_convert_fusion.select_ref
  86.3 0.8 fusion.116
  87.1 21.5 %all-gather.14.cloned.1.call-done = f32[4,258,256]{2,1,0:T(8,128)} async-done(((f32[1,258,256]{2,1,0:T(8,128)}), f32[4,258,256]{2,1,0:T(8,128)}) %all-gather.14.cloned.1.call-update) | async-done | bytes 1056784 | tf_op jit(solution)/shard_map/all_gather | solution.py:35
  108.6 0.8 fusion.118
  110.0 1.3 fusion.115
  111.3 1.6 multiply_add_fusion
  112.9 0.5 fusion.18
  113.4 0.8 multiply_reduce_fusion
  114.5 0.6 mul.762
  115.2 0.8 copy.58
  116.2 0.4 multiply_convert_fusion
  116.8 4.2 %all_to_all.19 = bf16[2,256,512]{1,2,0:T(8,128)(2,1)S(1)} all-to-all(bf16[2,256,512]{1,2,0:T(8,128)(2,1)S(1)} %copy.60), channel_id=1, replica_groups=mesh['sp_0'=4,'sp_1'=4,'sp_2'=4,'tp'=2] {'tp'}, dimensions={0} | all-to-all | bytes 1048576 | tf_op jit(solution)/shard_map/all_to_all | solution.py:402
  121.0 3.6 %fusion.9 = (f32[256]{0:T(256)S(1)}, bf16[256,2048]{1,0:T(8,128)(2,1)S(1)}) fusion(bf16[256,1024]{0,1:T(8,128)(2,1)S(1)} %bitcast.492, bf16[1024,2048]{1,0:T(8,128)(2,1)} %param.24, bf16[256,2048]{1,0:T(8,128)(2,1)S(1)} %copy-done.31), kind=kOutput, calls=%fused_computation.23 | convolution fusion | flops 1076887296 | bytes 6816768 | tf_op jit(solution)/shard_map/dot_general | solution.py:403
  124.6 1.3 fusion.11.normed_ref
  125.9 121.4 %shard_map.145 = bf16[256,2048]{1,0:T(8,128)(2,1)} custom-call(bf16[1024,256]{1,0:T(8,128)(2,1)} %or_convert_fusion.select_ref, bf16[2,256,1024]{2,1,0:T(8,128)(2,1)} %pad_maximum_fusion.weigh_ref, bf16[256,2048]{1,0:T(8,128)(2,1)} %fusion.11.normed_ref, bf16[256,2048]{1,0:T(8,128)(2,1)} %copy-done, bf16[2048,384]{1,0:T(8,128)(2,1)} %bitcast.476, ...), custom_call_target="tpu_custom_call" | custom-call | tf_op jit(solution)/shard_map/pallas_call | solution.py:248
  247.3 2.3 copy.145
  (222 shorter events, 8.2 us)
Async XLA Ops:
  6.5 3.7 %copy-start.5 = (bf16[512,512]{1,0:T(8,128)(2,1)S(1)}, bf16[512,512]{1,0:T(8,128)(2,1)}, u32[]{:S(2)}) copy-start(bf16[512,512]{1,0:T(8,128)(2,1)} %param.20) | copy-start | bytes 1572868
  6.5 43.2 %all-gather.10.cloned.1.call-start = ((), (), s32[]{:S(2)}) async-start(), calls=%async_computation.1 | async-start | bytes 1351680 | tf_op jit(solution)/shard_map/all_gather | solution.py:35
  22.1 32.0 %copy-start.7 = (bf16[512,256]{1,0:T(8,128)(2,1)S(1)}, bf16[512,256]{1,0:T(8,128)(2,1)}, u32[]{:S(2)}) copy-start(bf16[512,256]{1,0:T(8,128)(2,1)} %param.18) | copy-start | bytes 786436
  22.1 32.1 %copy-start.28 = (s32[64,1]{0,1:T(1,128)S(1)}, s32[64,1]{0,1:T(1,128)}, u32[]{:S(2)}) copy-start(s32[64,1]{0,1:T(1,128)} %constant.113) | copy-start | bytes 772
  22.1 32.1 %copy-start.29 = (s32[64,1]{0,1:T(1,128)S(1)}, s32[64,1]{0,1:T(1,128)}, u32[]{:S(2)}) copy-start(s32[64,1]{0,1:T(1,128)} %constant.114) | copy-start | bytes 772
  22.1 32.1 %copy-start.30 = (s32[64,1]{0,1:T(1,128)S(1)}, s32[64,1]{0,1:T(1,128)}, u32[]{:S(2)}) copy-start(s32[64,1]{0,1:T(1,128)} %constant.115) | copy-start | bytes 772
  22.1 32.2 %copy-start.9 = (s32[256,2]{0,1:T(2,128)S(1)}, s32[256,2]{0,1:T(2,128)}, u32[]{:S(2)}) copy-start(s32[256,2]{0,1:T(2,128)} %param.29) | copy-start | bytes 6148
  22.9 55.8 %all-gather.12.cloned.1.call-start = ((), (), s32[]{:S(2)}) async-start(), calls=%async_computation.2 | async-start | bytes 1351680 | tf_op jit(solution)/shard_map/all_gather | solution.py:35
  50.6 1.1 copy-start.20
  50.6 29.0 %copy-start.21 = (f32[2]{0:T(128)}, f32[2]{0:T(128)S(1)}, u32[]{:S(2)}) copy-start(f32[2]{0:T(128)S(1)} %get-tuple-element.196) | copy-start | bytes 28
  50.7 29.5 %copy-start.22 = (f32[2]{0:T(128)}, f32[2]{0:T(128)S(1)}, u32[]{:S(2)}) copy-start(f32[2]{0:T(128)S(1)} %get-tuple-element.237) | copy-start | bytes 28
  50.7 0.5 copy-start.26
  53.2 30.4 %copy-start.25 = (f32[256,2]{0,1:T(2,128)S(1)}, f32[256,2]{0,1:T(2,128)}, u32[]{:S(2)}) copy-start(f32[256,2]{0,1:T(2,128)} %param.30) | copy-start | bytes 6148
  54.0 54.6 %all-gather.14.cloned.1.call-start = ((), (), s32[]{:S(2)}) async-start(), calls=%async_computation.3 | async-start | bytes 1351680 | tf_op jit(solution)/shard_map/all_gather | solution.py:35
  80.2 1.2 copy-start.10
  80.2 4.9 %copy-start.12 = (f32[2]{0:T(128)}, f32[2]{0:T(128)S(1)}, u32[]{:S(2)}) copy-start(f32[2]{0:T(128)S(1)} %get-tuple-element.186) | copy-start | bytes 28
  80.2 4.9 %copy-start.14 = (f32[2]{0:T(128)}, f32[2]{0:T(128)S(1)}, u32[]{:S(2)}) copy-start(f32[2]{0:T(128)S(1)} %get-tuple-element.233) | copy-start | bytes 28
  80.3 4.8 %copy-start.16 = (f32[2]{0:T(128)}, f32[2]{0:T(128)S(1)}, u32[]{:S(2)}) copy-start(f32[2]{0:T(128)S(1)} %get-tuple-element.188) | copy-start | bytes 28
  80.3 4.8 %copy-start.18 = (f32[2]{0:T(128)}, f32[2]{0:T(128)S(1)}, u32[]{:S(2)}) copy-start(f32[2]{0:T(128)S(1)} %get-tuple-element.234) | copy-start | bytes 28
  80.3 0.6 copy-start.27
  83.7 2.5 copy-start.1
  84.0 2.2 copy-start.2
  86.2 23.6 %copy-start.23 = (f32[2]{0:T(128)S(1)}, f32[2]{0:T(128)}, u32[]{:S(2)}) copy-start(f32[2]{0:T(128)} %get-tuple-element.239) | copy-start | bytes 28
  86.3 23.6 %copy-start.24 = (f32[2]{0:T(128)S(1)}, f32[2]{0:T(128)}, u32[]{:S(2)}) copy-start(f32[2]{0:T(128)} %get-tuple-element.240) | copy-start | bytes 28
  86.3 25.0 %copy-start.11 = (f32[2]{0:T(128)S(1)}, f32[2]{0:T(128)}, u32[]{:S(2)}) copy-start(f32[2]{0:T(128)} %copy-done.10) | copy-start | bytes 28
  86.3 25.0 %copy-start.13 = (f32[2]{0:T(128)S(1)}, f32[2]{0:T(128)}, u32[]{:S(2)}) copy-start(f32[2]{0:T(128)} %copy-done.12) | copy-start | bytes 28
  86.3 25.0 %copy-start.15 = (f32[2]{0:T(128)S(1)}, f32[2]{0:T(128)}, u32[]{:S(2)}) copy-start(f32[2]{0:T(128)} %copy-done.14) | copy-start | bytes 28
  86.3 25.0 %copy-start.17 = (f32[2]{0:T(128)S(1)}, f32[2]{0:T(128)}, u32[]{:S(2)}) copy-start(f32[2]{0:T(128)} %copy-done.16) | copy-start | bytes 28
  86.3 25.0 %copy-start.19 = (f32[2]{0:T(128)S(1)}, f32[2]{0:T(128)}, u32[]{:S(2)}) copy-start(f32[2]{0:T(128)} %copy-done.18) | copy-start | bytes 28
  109.7 1.6 copy-start.4
  111.2 1.7 copy-start.3
  115.1 1.0 copy-start.6
  116.2 4.8 %copy-start.31 = (bf16[256,2048]{1,0:T(8,128)(2,1)S(1)}, bf16[256,2048]{1,0:T(8,128)(2,1)}, u32[]{:S(2)}) copy-start(bf16[256,2048]{1,0:T(8,128)(2,1)} %param.17) | copy-start | bytes 3145732
  120.9 3.6 %copy-start.8 = (f32[2048]{0:T(1024)S(1)}, f32[2048]{0:T(1024)}, u32[]{:S(2)}) copy-start(f32[2048]{0:T(1024)} %param.25) | copy-start | bytes 24580
  124.6 1.3 copy-start
Sparse Core Ops, SparseCore 0:
  23.1 26.6 all-gather.9
  54.1 24.5 all-gather.11
  83.8 24.7 all-gather.13

commit v2 on v1

--- a/solution.py
+++ b/solution.py
@@ -9,62 +9,11 @@
 MESH = pl.DeviceIdType.MESH
 QK = 128
 V_DIM = 256
-BLOCK = 64
 SP = ("sp_0", "sp_1", "sp_2")
 SP_TP = ("sp_0", "sp_1", "sp_2", "tp")
 
 
 epsilon = 1e-06
-floor_level = -1e30
-
-
-def neutral_like(array, identity):
-    return jax.tree.map(
-        lambda a, e: jnp.broadcast_to(jnp.asarray(e, a.dtype), a.shape), array, identity
-    )
-
-
-def gathered_once(array, axis):
-    leaves = jax.tree.leaves(array)
-    sequence = sorted(range(len(leaves)), key=lambda k: -leaves[k].size)
-    width = (1, *leaves[sequence[0]].shape)[-1]
-    lines = [
-        jnp.pad(leaves[k].reshape(-1), (0, -leaves[k].size % width)).reshape(-1, width)
-        for k in sequence
-    ]
-    both, at, found = (lax.all_gather(jnp.concatenate(lines), axis), 0, {})
-    for k, line in zip(sequence, lines):
-        share = both[:, at : at + len(line)].reshape(len(both), -1)
-        found[k] = share[:, : leaves[k].size].reshape(-1, *leaves[k].shape)
-        at += len(line)
-    numbers = iter(range(len(leaves)))
-    return jax.tree.map(lambda _: found[next(numbers)], array)
-
-
-def prefix_by_axis(array, axes, combine, identity):
-    before = start = neutral_like(array, identity)
-    total = array
-    for axis in reversed(axes):
-        count, position = (lax.axis_size(axis), lax.axis_index(axis))
-        pieces = gathered_once(total, axis)
-        inside, total = (start, start)
-        for k in range(count):
-            passed = k < position
-            total = combine(total, jax.tree.map(lambda part: part[k], pieces))
-            inside = jax.tree.map(lambda new, old: jnp.where(passed, new, old), total, inside)
-        before = combine(inside, before)
-    return before
-
-
-def join_states(earlier, later):
-    early_state, early_level, early_decay = earlier
-    late_state, late_level, late_decay = later
-    level = jnp.maximum(late_decay + early_level, late_level)
-    state = (
-        early_state * jnp.exp(late_decay + early_level - level)[:, None, None]
-        + late_state * jnp.exp(late_level - level)[:, None, None]
-    )
-    return (state, level, early_decay + late_decay)
 
 
 OFFSETS = sorted(
@@ -300,6 +249,233 @@
     return select, jnp.stack([high, low])
 
 
+def others(here, act):
+    me = (here[0] * 4 + here[1]) * 4 + here[2]
+
+    def step(k, _):
+        d = lax.rem(me + k, 64)
+        act(d, (d // 16, lax.rem(d // 4, 4), lax.rem(d, 4), here[3]))
+        return 0
+
+    lax.fori_loop(1, 64, step, 0)
+
+
+def mixer_kernel(
+    query_ref,
+    key_ref,
+    value_ref,
+    out_gate_ref,
+    in_gate_ref,
+    forget_ref,
+    out_ref,
+    table,
+    columns,
+    local_num,
+    local_level,
+    scalars,
+    all_scalars,
+    pieces,
+    all_pieces,
+    carries,
+    carried,
+    outbox,
+    send_sem,
+    recv_sem,
+):
+    here = place()
+    core = here[3]
+    me = (here[0] * 4 + here[1]) * 4 + here[2]
+    partner = (here[0], here[1], here[2], 1 - core)
+    barrier = pltpu.get_barrier_semaphore()
+    others(
+        here,
+        lambda d, dev: pl.semaphore_signal(barrier, inc=1, device_id=dev, device_id_type=MESH),
+    )
+    pl.semaphore_signal(barrier, inc=1, device_id=partner, device_id_type=MESH)
+
+    length = query_ref.shape[0]
+    scale = QK ** (-0.5)
+    x = forget_ref[...]
+    u = jnp.exp(-jnp.abs(x))
+    small = u * (1.0 - u * (0.5 - u * (1.0 / 3.0 - u * 0.25)))
+    decay = jnp.minimum(x, 0.0) - jnp.where(u < 0.01, small, jnp.log(1.0 + u))
+    table[...] = jnp.zeros_like(table)
+    table[0:2, :] = decay
+    raw = table[0:8, :]
+    high = raw.astype(jnp.bfloat16).astype(jnp.float32)
+    middle = (raw - high).astype(jnp.bfloat16).astype(jnp.float32)
+    low = raw - high - middle
+    parts = jnp.concatenate([high, middle, low], axis=0).astype(jnp.bfloat16)
+    before = lax.broadcasted_iota(jnp.int32, (length, length), 0)
+    after = lax.broadcasted_iota(jnp.int32, (length, length), 1)
+    upper = jnp.where(before <= after, 1.0, 0.0).astype(jnp.bfloat16)
+    summed = jnp.dot(parts, upper, preferred_element_type=jnp.float32)
+    summed = summed[0:8] + summed[8:16] + summed[16:24]
+    table[0:2, :] = summed[0:2]
+    table[2:4, :] = in_gate_ref[...]
+    columns[...] = table[...].T
+    rows_a, peaks = [], []
+    for h in range(2):
+        row_a = table[2 + h : 3 + h, :] - table[h : h + 1, :]
+        peak = jnp.max(row_a, axis=1, keepdims=True)
+        closing = table[h : h + 1, length - 1 : length]
+        scalars[h : h + 1, :] = jnp.broadcast_to(closing + peak, (1, 128))
+        scalars[2 + h : 3 + h, :] = jnp.broadcast_to(closing, (1, 128))
+        rows_a.append(row_a)
+        peaks.append(peak)
+    pl.semaphore_wait(barrier, 64)
+
+    def copy(src, dst, lane, dev):
+        return pltpu.make_async_remote_copy(
+            src_ref=src,
+            dst_ref=dst,
+            send_sem=send_sem.at[lane],
+            recv_sem=recv_sem.at[lane],
+            device_id=dev,
+            device_id_type=MESH,
+        )
+
+    def landed(ref, sem):
+        span = ref.at[pl.ds(0, 63)]
+        pltpu.make_async_copy(span, span, sem).wait()
+
+    others(here, lambda d, dev: copy(scalars, all_scalars.at[me], 0, dev).start())
+    all_scalars[me] = scalars[...]
+    for h in range(2):
+        col_a = columns[:, 2 + h : 3 + h] - columns[:, h : h + 1]
+        weight = jnp.exp(col_a - peaks[h]) * scale
+        keys = (key_ref[:, h * QK : (h + 1) * QK].astype(jnp.float32) * weight).astype(jnp.bfloat16)
+        state = lax.dot_general(
+            keys,
+            value_ref[:, h * V_DIM : (h + 1) * V_DIM],
+            (((0,), (0,)), ((), ())),
+            preferred_element_type=jnp.float32,
+        )
+        for half in range(2):
+            at = h * 32 + half * 16
+            pieces[at : at + 16] = state[:, half * 128 : (half + 1) * 128].reshape(16, 8, 128)
+    others(here, lambda d, dev: copy(pieces.at[d], all_pieces.at[me], 1, dev).start())
+    all_pieces[me] = pieces[me]
+
+    step = 128
+    for h in range(2):
+        for r in range(length // step):
+            n = (r + 1) * step
+            rows = slice(r * step, n)
+            score = lax.dot_general(
+                query_ref[rows, h * QK : (h + 1) * QK],
+                key_ref[0:n, h * QK : (h + 1) * QK],
+                (((1,), (1,)), ((), ())),
+                preferred_element_type=jnp.float32,
+            )
+            t = lax.broadcasted_iota(jnp.int32, (step, n), 0) + r * step
+            s = lax.broadcasted_iota(jnp.int32, (step, n), 1)
+            log_inner = jnp.where(s <= t, columns[rows, h : h + 1] + rows_a[h][:, 0:n], -1e30)
+            level = jnp.max(log_inner, axis=1, keepdims=True)
+            score = (score * scale * jnp.exp(log_inner - level)).astype(jnp.bfloat16)
+            local_num[rows, h * V_DIM : (h + 1) * V_DIM] = jnp.dot(
+                score, value_ref[0:n, h * V_DIM : (h + 1) * V_DIM], preferred_element_type=jnp.float32
+            )
+            local_level[h, rows, :] = jnp.broadcast_to(level, (step, 128))
+
+    landed(all_scalars, recv_sem.at[0])
+
+    def climb(s, level):
+        new = jnp.maximum(all_scalars[s, 2:4, :] + level, all_scalars[s, 0:2, :])
+        return jnp.where(s < me, new, level)
+
+    anchor = lax.fori_loop(0, 64, climb, jnp.zeros((2, 128), jnp.float32))
+    landed(all_pieces, recv_sem.at[1])
+    head = me // 32
+
+    def scan(s, held):
+        state, level = held
+        carries[s] = state
+        late = all_scalars[s, pl.ds(head, 1), :]
+        moved = all_scalars[s, pl.ds(2 + head, 1), :] + level
+        new = jnp.maximum(moved, late)
+        state = state * jnp.exp(moved - new) + all_pieces[s] * jnp.exp(late - new)
+        return (state, new)
+
+    lax.fori_loop(0, 64, scan, (jnp.zeros((8, 128), jnp.float32), jnp.zeros((1, 128), jnp.float32)))
+    others(here, lambda d, dev: copy(carries.at[d], carried.at[me], 2, dev).start())
+    carried[me] = carries[me]
+    landed(carried, recv_sem.at[2])
+
+    span = length // 2
+
+    def finish(start, store):
+        rows = pl.ds(pl.multiple_of(start, span), span)
+        for h in range(2):
+            state = jnp.concatenate(
+                [
+                    carried[h * 32 + half * 16 : h * 32 + (half + 1) * 16].reshape(QK, 128)
+                    for half in range(2)
+                ],
+                axis=1,
+            ).astype(jnp.bfloat16)
+            wide = slice(h * V_DIM, (h + 1) * V_DIM)
+            from_state = jnp.dot(
+                query_ref[rows, h * QK : (h + 1) * QK], state, preferred_element_type=jnp.float32
+            )
+            log_inter = columns[rows, h : h + 1] + anchor[h : h + 1, 0:1]
+            level = local_level[h, rows, 0:1]
+            peak = jnp.maximum(log_inter, level)
+            number = (
+                jnp.exp(log_inter - peak) * from_state + jnp.exp(level - peak) * local_num[rows, wide]
+            )
+            scaled = number * lax.rsqrt(
+                jnp.mean(number * number, axis=1, keepdims=True) + epsilon
+            )
+            gate = jax.nn.sigmoid(out_gate_ref[rows, wide].astype(jnp.float32))
+            store(h, (scaled * gate).astype(jnp.bfloat16))
+
+    def to_partner(h, value):
+        outbox[:, h * V_DIM : (h + 1) * V_DIM] = value
+
+    def to_self(h, value):
+        start = pl.multiple_of(core * 2 * V_DIM + h * V_DIM, V_DIM)
+        out_ref[:, pl.ds(start, V_DIM)] = value
+
+    finish((1 - core) * span, to_partner)
+    mine = pl.ds(pl.multiple_of(core * 2 * V_DIM, 2 * V_DIM), 2 * V_DIM)
+    swap = copy(outbox, out_ref.at[:, mine], 3, partner)
+    swap.start()
+    finish(core * span, to_self)
+    swap.wait()
+    for ref, lane in ((all_scalars, 0), (all_pieces, 1), (carried, 2)):
+        landed(ref, send_sem.at[lane])
+
+
+def mixer(queries, key_rows, value_rows, out_gate, in_gate, forget_gate):
+    length = queries.shape[0]
+    vmem = pl.BlockSpec(memory_space=pltpu.VMEM)
+    f32 = jnp.float32
+    return pl.pallas_call(
+        mixer_kernel,
+        out_shape=jax.ShapeDtypeStruct((length // 2, 4 * V_DIM), jnp.bfloat16),
+        in_specs=[vmem] * 6,
+        out_specs=vmem,
+        scratch_shapes=[
+            pltpu.VMEM((128, length), f32),
+            pltpu.VMEM((length, 128), f32),
+            pltpu.VMEM((length, 2 * V_DIM), f32),
+            pltpu.VMEM((2, length, 128), f32),
+            pltpu.VMEM((4, 128), f32),
+            pltpu.VMEM((64, 4, 128), f32),
+        ]
+        + [pltpu.VMEM((64, 8, 128), f32)] * 4
+        + [
+            pltpu.VMEM((length // 2, 2 * V_DIM), jnp.bfloat16),
+            pltpu.SemaphoreType.DMA((4,)),
+            pltpu.SemaphoreType.DMA((4,)),
+        ],
+        compiler_params=pltpu.CompilerParams(
+            collective_id=0, has_side_effects=True, vmem_limit_bytes=32 << 20
+        ),
+    )(queries, key_rows, value_rows, out_gate, in_gate, forget_gate)
+
+
 def body(
     stream,
     queries,
@@ -316,90 +492,7 @@
     expert_ids,
     route_weights,
 ):
-    heads_here, length = in_gate.shape
-    blocks = length // BLOCK
-
-    def per_head(rows, size):
-        return (
-            rows.astype(jnp.float32).reshape(blocks, BLOCK, heads_here, size).transpose(2, 0, 1, 3)
-        )
-
-    query_blocks = per_head(queries, QK)
-    key_blocks = per_head(key_rows, QK) * QK ** (-0.5)
-    value_blocks = per_head(value_rows, V_DIM)
-    input_gate = in_gate.reshape(heads_here, blocks, BLOCK)
-    cumulative = jnp.cumsum(
-        jax.nn.log_sigmoid(forget_gate).reshape(heads_here, blocks, BLOCK), axis=-1
-    )
-    closing = cumulative[..., -1]
-    causal = jnp.tril(jnp.ones((BLOCK, BLOCK), dtype=bool))
-    log_inner = jnp.where(
-        causal,
-        cumulative[..., :, None] - cumulative[..., None, :] + input_gate[..., None, :],
-        -jnp.inf,
-    )
-    log_close = closing[..., None] - cumulative + input_gate
-
-    def advance(carry, inputs):
-        state, level, decay = carry
-        key_block, value_block, close_block, last_block = inputs
-        new_level = jnp.maximum(last_block + level, jnp.max(close_block, axis=-1))
-        weight = jnp.exp(close_block - new_level[:, None])
-        update = jnp.einsum("hl,hld,hle->hde", weight, key_block, value_block)
-        new_state = state * jnp.exp(last_block + level - new_level)[:, None, None] + update
-        return ((new_state, new_level, decay + last_block), (state, level, decay))
-
-    empty = (
-        jnp.zeros((heads_here, QK, V_DIM), jnp.float32),
-        jnp.full((heads_here,), floor_level, jnp.float32),
-        jnp.zeros((heads_here,), jnp.float32),
-    )
-    summary, before = lax.scan(
-        advance,
-        empty,
-        (
-            jnp.moveaxis(key_blocks, 1, 0),
-            jnp.moveaxis(value_blocks, 1, 0),
-            jnp.moveaxis(log_close, 1, 0),
-            closing.T,
-        ),
-    )
-    carried = prefix_by_axis(summary, SP, join_states, empty)
-    anchor = join_states(
-        (
-            jnp.zeros((heads_here, QK, V_DIM), jnp.float32),
-            jnp.zeros((heads_here,), jnp.float32),
-            jnp.zeros((heads_here,), jnp.float32),
-        ),
-        carried,
-    )
-    anchor_state, anchor_level, _ = anchor
-    block_states, block_levels, block_decays = before
-    levels = jnp.maximum(block_decays + anchor_level[None, :], block_levels)
-    states = (
-        anchor_state[None] * jnp.exp(block_decays + anchor_level[None, :] - levels)[..., None, None]
-        + block_states * jnp.exp(block_levels - levels)[..., None, None]
-    )
-    states = jnp.moveaxis(states, 0, 1)
-    levels = levels.T
-    log_inter = cumulative + levels[..., None]
-    peak = jnp.maximum(log_inter, jnp.max(log_inner, axis=-1))
-    scores = jnp.einsum("hntd,hnsd->hnts", query_blocks, key_blocks) * jnp.exp(
-        log_inner - peak[..., None]
-    )
-    from_state = jnp.einsum("hntd,hnde->hnte", query_blocks, states)
-    from_block = jnp.einsum("hnts,hnse->hnte", scores, value_blocks)
-    numerator = jnp.exp(log_inter - peak)[..., None] * from_state + from_block
-    numerator = numerator.transpose(1, 2, 0, 3).reshape(length, heads_here, V_DIM)
-    scaled = numerator * lax.rsqrt(
-        jnp.mean(numerator * numerator, axis=-1, keepdims=True) + epsilon
-    )
-    gated = scaled.reshape(length, heads_here * V_DIM) * jax.nn.sigmoid(
-        out_gate.astype(jnp.float32)
-    )
-    heads_out = gated.astype(jnp.bfloat16)
-    rows_here, model_width = stream.shape
-    token_heads = lax.all_to_all(heads_out, "tp", split_axis=0, concat_axis=1, tiled=True)
+    token_heads = mixer(queries, key_rows, value_rows, out_gate, in_gate, forget_gate)
     mix = jnp.dot(token_heads, out_proj, preferred_element_type=jnp.float32)
     middle = (stream.astype(jnp.float32) + mix).astype(jnp.bfloat16)
     middle_float = middle.astype(jnp.float32)

time: 258 us -> 170 us (0.66)
  waiting for transfers between devices: 71.9 us -> 0 us
  Pallas kernels: 121 us -> 148 us
  other arithmetic: 22.3 us -> 5.29 us
  between operations: 13.9 us -> 0.1 us
  local copies, waits for them, and re-layouts: 14.2 us -> 9.27 us
  blocking collectives: 4.15 us -> 0 us
  matrix products: 7.81 us -> 3.91 us
    all_gather x3 -> x0, waiting for transfers between devices: 71.9 us -> none  [gathered_once(): both, at, found = (lax.all_gather(jnp.concatenate(lines), axis), 0, {})]
    pallas_call x0 -> x1, Pallas kernels: none -> 27.5 us  [mixer(): pl.pallas_call(mixer_kernel, out_shape=jax.ShapeDtypeStruct((length // 2,...]
    dynamic_update_slice x8 -> x0, other arithmetic: 5.92 us -> none  [body(): lax.scan(advance, empty, (jnp.moveaxis(key_blocks, 1, 0), jnp.moveaxis(va...]
    slice x7 -> x0, local copies, waits for them, and re-layouts: 4.86 us -> none  [the longest x3 2.54 us: gathered_once(): share = both[:, at:at + len(line)].reshape(len(both), -1)]
    add x12 -> x0, other arithmetic: 4.82 us -> none  [the longest x3 4.65 us: join_states(): early_state * jnp.exp(late_decay + early_level - level)[:, None, None]]
    all_to_all x1 -> x0, blocking collectives: 4.15 us -> none  [body(): lax.all_to_all(heads_out, 'tp', split_axis=0, concat_axis=1, tiled=True)]
    unnamed x72 -> x19, local copies, waits for them, and re-layouts: 3.74 us -> 7.67 us
    dot_general x10 -> x0, matrix products: 3.92 us -> none  [the longest x8 2.57 us: advance(): update = jnp.einsum('hl,hld,hle->hde', weight, key_block, value_block)]
  transfers between devices with their start and end apart: 3 -> 0, of which waited for: 3 -> 0; matrix products, arithmetic and copies ran while one was open for 2% -> 0% of each run, Pallas kernels for 0% -> 0%
where the time goes in v2:
time: 170 us; the launch traced here: 167 us
  Pallas kernels  148 us (87%)
  local copies, waits for them, and re-layouts  9.27 us (5%)
  other arithmetic  5.29 us (3%)
  matrix products  3.91 us (2%)
    pallas_call x1, Pallas kernels, experts(): pl.pallas_call(experts_kernel, out_shape=jax.ShapeDtypeStruct((rows_here,...  120 us
    pallas_call x1, Pallas kernels, mixer(): pl.pallas_call(mixer_kernel, out_shape=jax.ShapeDtypeStruct((length // 2,...  27.5 us
    unnamed x19, local copies, waits for them, and re-layouts  7.67 us
    dot_general x1, matrix products, body(): mix = jnp.dot(token_heads, out_proj, preferred_element_type=jnp.float32)  3.64 us

profile of v2, /device:TPU:0, one launch (start us, length us, event | category | flops | bytes accessed | tf_op | source)
XLA Modules:
  0.0 166.5 jit_solution(3993978106529446075)
XLA Ops:
  0.0 0.0 copy-start.8
  0.0 0.8 fusion.24
  0.8 0.8 fusion.29
  1.6 0.8 fusion.30
  2.3 0.3 select_reduce_fusion.1
  2.6 0.8 multiply_add_fusion.1
  3.4 0.1 iota_add_fusion
  3.5 0.1 add.124
  3.6 1.0 or_convert_fusion.select_ref
  4.6 0.0 copy-start
  4.6 1.0 copy-done
  5.6 0.0 copy-start.1
  5.6 1.0 copy-done.1
  6.6 0.0 copy-start.2
  6.6 0.9 copy-done.2
  7.6 0.0 copy-start.3
  7.6 0.9 copy-done.3
  8.5 0.0 copy-start.4
  8.5 0.7 copy-done.4
  9.2 0.0 copy-start.5
  9.2 0.7 copy-done.5
  9.9 27.5 %shard_map.145 = bf16[256,1024]{1,0:T(8,128)(2,1)S(1)} custom-call(bf16[512,256]{1,0:T(8,128)(2,1)S(1)} %copy-done.2, bf16[512,256]{1,0:T(8,128)(2,1)S(1)} %copy-done.3, bf16[512,512]{1,0:T(8,128)(2,1)S(1)} %copy-done, bf16[512,512]{1,0:T(8,128)(2,1)S(1)} %copy-done.1, f32[2,512]{1,0:T(2,128)S(1)} %copy-done.4, f32[2,512]{1,0:T(2,128)S(1)} %copy-done.5), custom_call_target="tpu_custom_call" | custom-call | tf_op jit(solution)/shard_map/pallas_call | solution.py:454
  37.4 0.0 copy-done.8
  37.4 3.6 %fusion.1 = (f32[256]{0:T(256)S(1)}, bf16[256,2048]{1,0:T(8,128)(2,1)S(1)}) fusion(bf16[256,1024]{1,0:T(8,128)(2,1)S(1)} %shard_map.145, bf16[1024,2048]{1,0:T(8,128)(2,1)} %param.22, bf16[256,2048]{1,0:T(8,128)(2,1)S(1)} %copy-done.8), kind=kOutput, calls=%fused_computation.4 | convolution fusion | flops 1076887296 | bytes 6816768 | tf_op jit(solution)/shard_map/dot_general | solution.py:496
  41.0 0.0 copy-start.6
  41.0 0.0 copy-start.7
  41.1 0.3 fusion.4
  41.4 1.1 pad_maximum_fusion.weigh_ref
  42.4 0.0 copy-done.7
  42.4 1.3 fusion.3.normed_ref
  43.7 0.0 copy-done.6
  43.7 120.5 %shard_map.146 = bf16[256,2048]{1,0:T(8,128)(2,1)} custom-call(bf16[1024,256]{1,0:T(8,128)(2,1)} %or_convert_fusion.select_ref, bf16[2,256,1024]{2,1,0:T(8,128)(2,1)} %pad_maximum_fusion.weigh_ref, bf16[256,2048]{1,0:T(8,128)(2,1)} %fusion.3.normed_ref, bf16[256,2048]{1,0:T(8,128)(2,1)} %copy-done.6, bf16[2048,384]{1,0:T(8,128)(2,1)} %bitcast.15, ...), custom_call_target="tpu_custom_call" | custom-call | tf_op jit(solution)/shard_map/pallas_call | solution.py:197
  164.2 2.3 %copy.17 = bf16[256,2048]{1,0:T(8,128)(2,1)} copy(bf16[256,2048]{1,0:T(8,128)(2,1)} %shard_map.146) | data formatting | bytes 2097152
  (5 shorter events, 0.0 us)
Async XLA Ops:
  0.0 37.4 %copy-start.8 = (bf16[256,2048]{1,0:T(8,128)(2,1)S(1)}, bf16[256,2048]{1,0:T(8,128)(2,1)}, u32[]{:S(2)}) copy-start(bf16[256,2048]{1,0:T(8,128)(2,1)} %param.15) | copy-start | bytes 3145732
  4.6 1.0 copy-start
  5.6 1.0 copy-start.1
  6.6 0.9 copy-start.2
  7.6 0.9 copy-start.3
  8.5 0.7 copy-start.4
  9.2 0.7 copy-start.5
  41.0 2.7 %copy-start.6 = (bf16[256,2048]{1,0:T(8,128)(2,1)}, bf16[256,2048]{1,0:T(8,128)(2,1)S(1)}, u32[]{:S(2)}) copy-start(bf16[256,2048]{1,0:T(8,128)(2,1)S(1)} %get-tuple-element.16.middle_ref) | copy-start | bytes 3145732
  41.0 1.4 copy-start.7

commit v3 on v2

v3 whole, which is shorter than its diff:
```python
import jax
import jax.numpy as jnp
from jax import lax
from jax.experimental import pallas as pl
from jax.experimental.pallas import tpu as pltpu
from jax.sharding import Mesh
from jax.sharding import PartitionSpec as P

MESH = pl.DeviceIdType.MESH
QK = 128
V_DIM = 256
SP = ("sp_0", "sp_1", "sp_2")
SP_TP = ("sp_0", "sp_1", "sp_2", "tp")
SLOT = 16
GROUP_ROWS = 256
PER_GROUP = GROUP_ROWS // SLOT
TILE = 256
epsilon = 1e-06
F32 = jnp.float32
BF16 = jnp.bfloat16


def offsets_by_orbit():
    cube = [(a, b, c) for a in range(4) for b in range(4) for c in range(4)]
    seen, orbits = {(0, 0, 0)}, []
    for o in sorted(cube, key=lambda o: sum(min(v, 4 - v) for v in o)):
        orbit = []
        for turn in range(3):
            turned = o[turn:] + o[:turn]
            for p in (turned, tuple(-v % 4 for v in turned)):
                if p not in seen:
                    seen.add(p)
                    orbit.append(p)
        if orbit:
            orbits.append(orbit)
    order = [(0, 0, 0)]
    while orbits:
        order += orbits.pop(0)
        if orbits:
            order += orbits.pop()
    return order


OFFSETS = offsets_by_orbit()
GROUPS = len(OFFSETS) // PER_GROUP


def place():
    return [lax.axis_index(axis) for axis in SP_TP]


def peer(here, offset, sign=1):
    z, y, x, core = here
    return tuple(lax.rem(p + (sign * o) % 4, 4) for p, o in zip((z, y, x), offset)) + (core,)


def index_of(device):
    return (device[0] * 4 + device[1]) * 4 + device[2]


def others(here, act):
    me = index_of(here)

    def step(k, _):
        d = lax.rem(me + k, 64)
        act(d, (d // 16, lax.rem(d // 4, 4), lax.rem(d, 4), here[3]))
        return 0

    lax.fori_loop(1, 64, step, 0)


def route(ids_ref, routes_ref, pairs, ranks, shares, select_ref, weigh_ref, here, loads):
    loads["ids"].wait()
    loads["routes"].wait()
    pairs[...] = jnp.zeros_like(pairs)
    pairs[:, 0:2] = ids_ref[...].astype(F32)
    pairs[:, 2:4] = routes_ref[...]
    turned = pairs[...].T
    tokens = turned.shape[1]
    expert = lax.broadcasted_iota(jnp.int32, (len(OFFSETS), tokens), 0).astype(F32)
    first, second = (turned[j : j + 1, :] == expert for j in range(2))
    used = jnp.where(first | second, 1.0, 0.0)
    earlier = lax.broadcasted_iota(jnp.int32, (tokens, tokens), 0)
    later = lax.broadcasted_iota(jnp.int32, (tokens, tokens), 1)
    upper = jnp.where(earlier < later, 1.0, 0.0).astype(BF16)
    rank = jnp.dot(used.astype(BF16), upper, preferred_element_type=F32)
    ranks[...] = jnp.where(first | second, rank, -1.0)
    shares[...] = jnp.where(first, turned[2:3, :], 0.0) + jnp.where(second, turned[3:4, :], 0.0)
    slot = lax.broadcasted_iota(jnp.int32, (SLOT, tokens), 0).astype(F32)
    for g in range(GROUPS):
        weights = []
        for i in range(g * PER_GROUP, (g + 1) * PER_GROUP):
            owner = pl.ds(index_of(peer(here, OFFSETS[i])), 1)
            chosen = ranks[owner, :] == slot
            select_ref[pl.ds(i * SLOT, SLOT), :] = jnp.where(chosen, 1.0, 0.0).astype(BF16)
            weights.append(jnp.where(chosen, shares[owner, :], 0.0))
        weigh = jnp.concatenate(weights, axis=0).T
        high = weigh.astype(BF16)
        cols = slice(g * GROUP_ROWS, (g + 1) * GROUP_ROWS)
        weigh_ref[0, :, cols] = high
        weigh_ref[1, :, cols] = (weigh - high.astype(F32)).astype(BF16)


def layer_kernel(
    stream_hbm,
    query_hbm,
    key_hbm,
    value_hbm,
    out_gate_hbm,
    in_gate_hbm,
    forget_hbm,
    out_proj_hbm,
    gain_hbm,
    gate_ref,
    up_ref,
    down_ref,
    ids_hbm,
    routes_hbm,
    out_ref,
    stream_ref,
    query_ref,
    key_ref,
    value_ref,
    out_gate_ref,
    in_gate_ref,
    forget_ref,
    out_proj_ref,
    gain_ref,
    ids_ref,
    routes_ref,
    table,
    columns,
    local_num,
    local_level,
    scalars,
    all_scalars,
    pieces,
    all_pieces,
    carries,
    carried,
    outbox,
    heads,
    pairs,
    ranks,
    shares,
    select_ref,
    weigh_ref,
    middle_ref,
    normed_ref,
    outgoing,
    arrived,
    answers,
    returned,
    gate_full,
    up_full,
    down_full,
    hidden,
    total,
    load_sem,
    send_sem,
    recv_sem,
    weight_send,
    weight_recv,
    rows_send,
    rows_recv,
    back_send,
    back_recv,
):
    here = place()
    core = here[3]
    me = index_of(here)
    partner = (here[0], here[1], here[2], 1 - core)
    units = gate_ref.shape[1]
    loads = {}
    for name, src, dst in (
        ("forget", forget_hbm, forget_ref),
        ("in", in_gate_hbm, in_gate_ref),
        ("key", key_hbm, key_ref),
        ("value", value_hbm, value_ref),
        ("query", query_hbm, query_ref),
        ("ids", ids_hbm, ids_ref),
        ("routes", routes_hbm, routes_ref),
        ("out_gate", out_gate_hbm, out_gate_ref),
        ("out_proj", out_proj_hbm, out_proj_ref),
        ("stream", stream_hbm, stream_ref),
        ("gain", gain_hbm, gain_ref),
        ("gate", gate_ref, gate_full.at[:, pl.ds(0, units)]),
        ("up", up_ref, up_full.at[:, pl.ds(0, units)]),
        ("down", down_ref, down_full.at[pl.ds(0, units)]),
    ):
        loads[name] = pltpu.make_async_copy(src, dst, load_sem.at[len(loads)])
        loads[name].start()
    barrier = pltpu.get_barrier_semaphore()
    others(
        here,
        lambda d, dev: pl.semaphore_signal(barrier, inc=1, device_id=dev, device_id_type=MESH),
    )
    pl.semaphore_signal(barrier, inc=1, device_id=partner, device_id_type=MESH)

    length = query_ref.shape[0]
    scale = QK ** (-0.5)
    loads["forget"].wait()
    loads["in"].wait()
    x = forget_ref[...]
    u = jnp.exp(-jnp.abs(x))
    small = u * (1.0 - u * (0.5 - u * (1.0 / 3.0 - u * 0.25)))
    decay = jnp.minimum(x, 0.0) - jnp.where(u < 0.01, small, jnp.log(1.0 + u))
    table[...] = jnp.zeros_like(table)
    table[0:2, :] = decay
    raw = table[0:8, :]
    high = raw.astype(jnp.bfloat16).astype(jnp.float32)
    mid = (raw - high).astype(jnp.bfloat16).astype(jnp.float32)
    low = raw - high - mid
    parts = jnp.concatenate([high, mid, low], axis=0).astype(jnp.bfloat16)
    before = lax.broadcasted_iota(jnp.int32, (length, length), 0)
    after = lax.broadcasted_iota(jnp.int32, (length, length), 1)
    upper = jnp.where(before <= after, 1.0, 0.0).astype(jnp.bfloat16)
    summed = jnp.dot(parts, upper, preferred_element_type=jnp.float32)
    summed = summed[0:8] + summed[8:16] + summed[16:24]
    table[0:2, :] = summed[0:2]
    table[2:4, :] = in_gate_ref[...]
    columns[...] = table[...].T
    rows_a, peaks = [], []
    for h in range(2):
        row_a = table[2 + h : 3 + h, :] - table[h : h + 1, :]
        peak = jnp.max(row_a, axis=1, keepdims=True)
        closing = table[h : h + 1, length - 1 : length]
        scalars[h : h + 1, :] = jnp.broadcast_to(closing + peak, (1, 128))
        scalars[2 + h : 3 + h, :] = jnp.broadcast_to(closing, (1, 128))
        rows_a.append(row_a)
        peaks.append(peak)
    pl.semaphore_wait(barrier, 64)

    def copy(src, dst, lane, dev):
        return pltpu.make_async_remote_copy(
            src_ref=src,
            dst_ref=dst,
            send_sem=send_sem.at[lane],
            recv_sem=recv_sem.at[lane],
            device_id=dev,
            device_id_type=MESH,
        )

    def landed(ref, sem):
        span = ref.at[pl.ds(0, 63)]
        pltpu.make_async_copy(span, span, sem).wait()

    others(here, lambda d, dev: copy(scalars, all_scalars.at[me], 0, dev).start())
    all_scalars[me] = scalars[...]
    loads["key"].wait()
    loads["value"].wait()
    for h in range(2):
        col_a = columns[:, 2 + h : 3 + h] - columns[:, h : h + 1]
        weight = jnp.exp(col_a - peaks[h]) * scale
        keys = (key_ref[:, h * QK : (h + 1) * QK].astype(jnp.float32) * weight).astype(jnp.bfloat16)
        state = lax.dot_general(
            keys,
            value_ref[:, h * V_DIM : (h + 1) * V_DIM],
            (((0,), (0,)), ((), ())),
            preferred_element_type=jnp.float32,
        )
        for half in range(2):
            at = h * 32 + half * 16
            pieces[at : at + 16] = state[:, half * 128 : (half + 1) * 128].reshape(16, 8, 128)
    others(here, lambda d, dev: copy(pieces.at[d], all_pieces.at[me], 1, dev).start())
    all_pieces[me] = pieces[me]

    loads["query"].wait()
    step = 128
    for h in range(2):
        for r in range(length // step):
            n = (r + 1) * step
            rows = slice(r * step, n)
            score = lax.dot_general(
                query_ref[rows, h * QK : (h + 1) * QK],
                key_ref[0:n, h * QK : (h + 1) * QK],
                (((1,), (1,)), ((), ())),
                preferred_element_type=jnp.float32,
            )
            t = lax.broadcasted_iota(jnp.int32, (step, n), 0) + r * step
            s = lax.broadcasted_iota(jnp.int32, (step, n), 1)
            log_inner = jnp.where(s <= t, columns[rows, h : h + 1] + rows_a[h][:, 0:n], -1e30)
            level = jnp.max(log_inner, axis=1, keepdims=True)
            score = (score * scale * jnp.exp(log_inner - level)).astype(jnp.bfloat16)
            local_num[rows, h * V_DIM : (h + 1) * V_DIM] = jnp.dot(
                score, value_ref[0:n, h * V_DIM : (h + 1) * V_DIM], preferred_element_type=jnp.float32
            )
            local_level[h, rows, :] = jnp.broadcast_to(level, (step, 128))

    landed(all_scalars, recv_sem.at[0])

    def climb(s, level):
        new = jnp.maximum(all_scalars[s, 2:4, :] + level, all_scalars[s, 0:2, :])
        return jnp.where(s < me, new, level)

    anchor = lax.fori_loop(0, 64, climb, jnp.zeros((2, 128), jnp.float32))
    landed(all_pieces, recv_sem.at[1])
    head = me // 32

    def scan(s, held):
        state, level = held
        carries[s] = state
        late = all_scalars[s, pl.ds(head, 1), :]
        moved = all_scalars[s, pl.ds(2 + head, 1), :] + level
        new = jnp.maximum(moved, late)
        state = state * jnp.exp(moved - new) + all_pieces[s] * jnp.exp(late - new)
        return (state, new)

    lax.fori_loop(0, 64, scan, (jnp.zeros((8, 128), jnp.float32), jnp.zeros((1, 128), jnp.float32)))
    others(here, lambda d, dev: copy(carries.at[d], carried.at[me], 2, dev).start())
    carried[me] = carries[me]
    route(ids_ref, routes_ref, pairs, ranks, shares, select_ref, weigh_ref, here, loads)
    landed(carried, recv_sem.at[2])

    span = length // 2

    def finish(start, store):
        rows = pl.ds(pl.multiple_of(start, span), span)
        for h in range(2):
            state = jnp.concatenate(
                [
                    carried[h * 32 + half * 16 : h * 32 + (half + 1) * 16].reshape(QK, 128)
                    for half in range(2)
                ],
                axis=1,
            ).astype(jnp.bfloat16)
            wide = slice(h * V_DIM, (h + 1) * V_DIM)
            from_state = jnp.dot(
                query_ref[rows, h * QK : (h + 1) * QK], state, preferred_element_type=jnp.float32
            )
            log_inter = columns[rows, h : h + 1] + anchor[h : h + 1, 0:1]
            level = local_level[h, rows, 0:1]
            peak = jnp.maximum(log_inter, level)
            number = (
                jnp.exp(log_inter - peak) * from_state + jnp.exp(level - peak) * local_num[rows, wide]
            )
            scaled = number * lax.rsqrt(
                jnp.mean(number * number, axis=1, keepdims=True) + epsilon
            )
            gate = jax.nn.sigmoid(out_gate_ref[rows, wide].astype(jnp.float32))
            store(h, (scaled * gate).astype(jnp.bfloat16))

    def to_partner(h, value):
        outbox[:, h * V_DIM : (h + 1) * V_DIM] = value

    def to_self(h, value):
        start = pl.multiple_of(core * 2 * V_DIM + h * V_DIM, V_DIM)
        heads[:, pl.ds(start, V_DIM)] = value

    loads["out_gate"].wait()
    finish((1 - core) * span, to_partner)
    mine = pl.ds(pl.multiple_of(core * 2 * V_DIM, 2 * V_DIM), 2 * V_DIM)
    swap = copy(outbox, heads.at[:, mine], 3, partner)
    swap.start()
    weights = [
        pltpu.make_async_remote_copy(
            src_ref=mine_,
            dst_ref=theirs,
            send_sem=weight_send.at[i],
            recv_sem=weight_recv.at[i],
            device_id=partner,
            device_id_type=MESH,
        )
        for i, (mine_, theirs) in enumerate(
            (
                (gate_ref, gate_full.at[:, pl.ds(units, units)]),
                (up_ref, up_full.at[:, pl.ds(units, units)]),
                (down_ref, down_full.at[pl.ds(units, units)]),
            )
        )
    ]
    for weight in weights:
        weight.start()
    finish(core * span, to_self)
    swap.wait()
    loads["out_proj"].wait()
    loads["stream"].wait()
    loads["gain"].wait()
    width = stream_ref.shape[1]
    tiles = [slice(n, n + TILE) for n in range(0, width, TILE)]
    squares = jnp.zeros((stream_ref.shape[0], 1), F32)
    for cols in tiles:
        mix = jnp.dot(heads[...], out_proj_ref[:, cols], preferred_element_type=F32)
        both = (stream_ref[:, cols].astype(F32) + mix).astype(BF16)
        middle_ref[:, cols] = both
        both = both.astype(F32)
        squares = squares + jnp.sum(both * both, axis=1, keepdims=True)
    factor = lax.rsqrt(squares / width + epsilon)
    for cols in tiles:
        normed_ref[:, cols] = (middle_ref[:, cols].astype(F32) * factor * gain_ref[:, cols]).astype(BF16)

    def rows(i):
        return pl.ds(i * SLOT, SLOT)

    def group(g):
        return pl.ds(g * GROUP_ROWS, GROUP_ROWS)

    def members(g):
        return range(max(g * PER_GROUP, 1), (g + 1) * PER_GROUP)

    def build(g):
        pick = select_ref[group(g), :]
        for cols in tiles:
            outgoing[group(g), cols] = jnp.dot(
                pick, normed_ref[:, cols], preferred_element_type=F32
            ).astype(BF16)

    def send(g):
        for i in members(g):
            pltpu.make_async_remote_copy(
                src_ref=outgoing.at[rows(i)],
                dst_ref=arrived.at[rows(i)],
                send_sem=rows_send,
                recv_sem=rows_recv.at[g],
                device_id=peer(here, OFFSETS[i]),
                device_id_type=MESH,
            ).start()

    build(0)
    for g in range(1, GROUPS):
        send(g - 1)
        build(g)
    arrived[rows(0), :] = outgoing[rows(0), :]
    send(GROUPS - 1)

    def all_in(ref, sem, first, last):
        span = ref.at[pl.ds(first * SLOT, (last - first) * SLOT)]
        pltpu.make_async_copy(span, span, sem).wait()

    for name in ("gate", "up", "down"):
        loads[name].wait()
    for weight in weights:
        weight.wait_recv()
    for g in range(GROUPS):
        all_in(arrived, rows_recv.at[g], members(g)[0], members(g)[-1] + 1)
        block = arrived[group(g), :]
        for n in range(0, hidden.shape[1], TILE):
            cols = slice(n, n + TILE)
            gates = jnp.dot(block, gate_full[:, cols], preferred_element_type=F32)
            ups = jnp.dot(block, up_full[:, cols], preferred_element_type=F32)
            hidden[:, cols] = (gates * jax.nn.sigmoid(gates) * ups).astype(BF16)
        for cols in tiles:
            answers[group(g), cols] = jnp.dot(
                hidden[...], down_full[:, cols], preferred_element_type=F32
            ).astype(BF16)
        for i in members(g):
            pltpu.make_async_remote_copy(
                src_ref=answers.at[rows(i)],
                dst_ref=returned.at[rows(i)],
                send_sem=back_send,
                recv_sem=back_recv.at[g],
                device_id=peer(here, OFFSETS[i], -1),
                device_id_type=MESH,
            ).start()
    returned[rows(0), :] = answers[rows(0), :]
    for g in range(GROUPS):
        all_in(returned, back_recv.at[g], members(g)[0], members(g)[-1] + 1)
        for cols in tiles:
            part = jnp.dot(
                weigh_ref[0, :, group(g)], returned[group(g), cols], preferred_element_type=F32
            ) + jnp.dot(
                weigh_ref[1, :, group(g)], returned[group(g), cols], preferred_element_type=F32
            )
            before = middle_ref[:, cols].astype(F32) if g == 0 else total[:, cols]
            if g < GROUPS - 1:
                total[:, cols] = before + part
            else:
                out_ref[:, cols] = (before + part).astype(out_ref.dtype)
    all_in(outgoing, rows_send, 1, len(OFFSETS))
    all_in(answers, back_send, 1, len(OFFSETS))
    for weight in weights:
        weight.wait_send()
    for ref, lane in ((all_scalars, 0), (all_pieces, 1), (carried, 2)):
        landed(ref, send_sem.at[lane])


def body(*arrays):
    (
        stream,
        queries,
        key_rows,
        value_rows,
        out_gate,
        in_gate,
        forget_gate,
        out_proj,
        ffn_gain,
        gate_proj,
        up_proj,
        down_proj,
        expert_ids,
        route_weights,
    ) = arrays
    rows_here, width = stream.shape
    length = queries.shape[0]
    half = gate_proj.shape[2]
    slots = len(OFFSETS) * SLOT
    gain = ffn_gain.reshape(1, width)
    loaded = [
        stream,
        queries,
        key_rows,
        value_rows,
        out_gate,
        in_gate,
        forget_gate,
        out_proj,
        gain,
        expert_ids,
        route_weights,
    ]
    vmem, dma = pltpu.VMEM, pltpu.SemaphoreType.DMA
    return pl.pallas_call(
        layer_kernel,
        out_shape=jax.ShapeDtypeStruct((rows_here, width), BF16),
        in_specs=[pl.BlockSpec(memory_space=pl.ANY)] * 14,
        out_specs=pl.BlockSpec(memory_space=pltpu.VMEM),
        scratch_shapes=[vmem(a.shape, a.dtype) for a in loaded]
        + [
            vmem((128, length), F32),
            vmem((length, 128), F32),
            vmem((length, 2 * V_DIM), F32),
            vmem((2, length, 128), F32),
            vmem((4, 128), F32),
            vmem((64, 4, 128), F32),
        ]
        + [vmem((64, 8, 128), F32)] * 4
        + [
            vmem((rows_here, 2 * V_DIM), BF16),
            vmem((rows_here, 4 * V_DIM), BF16),
            vmem((rows_here, 128), F32),
            vmem((len(OFFSETS), rows_here), F32),
            vmem((len(OFFSETS), rows_here), F32),
            vmem((slots, rows_here), BF16),
            vmem((2, rows_here, slots), BF16),
            vmem((rows_here, width), BF16),
            vmem((rows_here, width), BF16),
        ]
        + [vmem((slots, width), BF16)] * 4
        + [
            vmem((width, 2 * half), BF16),
            vmem((width, 2 * half), BF16),
            vmem((2 * half, width), BF16),
            vmem((GROUP_ROWS, 2 * half), BF16),
            vmem((rows_here, width), F32),
            dma((14,)),
            dma((4,)),
            dma((4,)),
            dma((3,)),
            dma((3,)),
            dma(()),
            dma((GROUPS,)),
            dma(()),
            dma((GROUPS,)),
        ],
        compiler_params=pltpu.CompilerParams(
            collective_id=0, has_side_effects=True, vmem_limit_bytes=62 << 20
        ),
    )(
        stream,
        queries,
        key_rows,
        value_rows,
        out_gate,
        in_gate,
        forget_gate,
        out_proj,
        gain,
        gate_proj[0],
        up_proj[0],
        down_proj[0],
        expert_ids,
        route_weights,
    )


def solution(mesh):
    split = Mesh(mesh.devices.reshape(4, 4, 4, mesh.shape["tp"]), ("sp_0", "sp_1", "sp_2", "tp"))
    return jax.shard_map(
        body,
        mesh=split,
        in_specs=(
            P(SP_TP, None),
            P(SP, "tp"),
            P(SP, "tp"),
            P(SP, "tp"),
            P(SP, "tp"),
            P("tp", SP),
            P("tp", SP),
            P(),
            P(),
            P(SP, None, "tp"),
            P(SP, None, "tp"),
            P(SP, "tp", None),
            P(SP_TP, None),
            P(SP_TP, None),
        ),
        out_specs=P(SP_TP, None),
        check_vma=False,
    )
```

time: 170 us -> 150 us (0.88)
  other arithmetic: 5.29 us -> 0 us
  Pallas kernels: 148 us -> 143 us
  local copies, waits for them, and re-layouts: 9.27 us -> 5.24 us
  matrix products: 3.91 us -> 0 us
    pallas_call x2 -> x1, Pallas kernels: 148 us -> 143 us  [body(): pl.pallas_call(layer_kernel, out_shape=jax.ShapeDtypeStruct((rows_here, w...]
    dot_general x2 -> x0, matrix products: 3.91 us -> none  [the longest x1 3.64 us: body(): mix = jnp.dot(token_heads, out_proj, preferred_element_type=jnp.float32)]
    convert_element_type x5 -> x0, other arithmetic: 2.59 us -> none  [the longest x1 1.27 us: body(): normed = (middle_float * lax.rsqrt(jnp.mean(middle_float * middle_float,...]
    unnamed x19 -> x3, local copies, waits for them, and re-layouts: 7.67 us -> 5.24 us
where the time goes in v3:
time: 150 us; the launch traced here: 148 us
  Pallas kernels  143 us (95%)
  local copies, waits for them, and re-layouts  5.24 us (3%)
    pallas_call x1, Pallas kernels, body(): pl.pallas_call(layer_kernel, out_shape=jax.ShapeDtypeStruct((rows_here, w...  143 us
    unnamed x3, local copies, waits for them, and re-layouts  5.24 us

profile of v3, /device:TPU:0, one launch (start us, length us, event | category | flops | bytes accessed | tf_op | source)
XLA Modules:
  0.0 148.1 jit_solution(14542992518496891605)
XLA Ops:
  0.0 1.5 copy.15.ids_hbm
  1.5 1.5 copy.16.routes_hbm
  2.9 142.8 %shard_map.136 = bf16[256,2048]{1,0:T(8,128)(2,1)} custom-call(bf16[256,2048]{1,0:T(8,128)(2,1)} %stream_hbm.1, bf16[512,256]{1,0:T(8,128)(2,1)} %query_hbm.1, bf16[512,256]{1,0:T(8,128)(2,1)} %key_hbm.1, bf16[512,512]{1,0:T(8,128)(2,1)} %value_hbm.1, bf16[512,512]{1,0:T(8,128)(2,1)} %out_gate_hbm.1, f32[2,512]{1,0:T(2,128)} %in_gate_hbm.1, ...), custom_call_target="tpu_custom_call" | custom-call | tf_op jit(solution)/shard_map/pallas_call | solution.py:513
  145.8 2.3 %copy.18 = bf16[256,2048]{1,0:T(8,128)(2,1)} copy(bf16[256,2048]{1,0:T(8,128)(2,1)} %shard_map.136) | data formatting | bytes 2097152

commit v4 on v3

--- a/solution.py
+++ b/solution.py
@@ -58,34 +58,29 @@
     return (device[0] * 4 + device[1]) * 4 + device[2]
 
 
+FAR_FIRST = sorted(OFFSETS[1:], key=lambda o: -sum(min(v, 4 - v) for v in o))
+
+
 def others(here, act):
-    me = index_of(here)
-
-    def step(k, _):
-        d = lax.rem(me + k, 64)
-        act(d, (d // 16, lax.rem(d // 4, 4), lax.rem(d, 4), here[3]))
-        return 0
-
-    lax.fori_loop(1, 64, step, 0)
-
-
-def route(ids_ref, routes_ref, pairs, ranks, shares, select_ref, weigh_ref, here, loads):
+    for offset in FAR_FIRST:
+        device = peer(here, offset)
+        act(index_of(device), device)
+
+
+def route(ids_ref, routes_ref, ranks, shares, select_ref, weigh_ref, here, loads):
     loads["ids"].wait()
     loads["routes"].wait()
-    pairs[...] = jnp.zeros_like(pairs)
-    pairs[:, 0:2] = ids_ref[...].astype(F32)
-    pairs[:, 2:4] = routes_ref[...]
-    turned = pairs[...].T
-    tokens = turned.shape[1]
+    named = ids_ref[...].astype(F32)
+    tokens = named.shape[1]
     expert = lax.broadcasted_iota(jnp.int32, (len(OFFSETS), tokens), 0).astype(F32)
-    first, second = (turned[j : j + 1, :] == expert for j in range(2))
+    first, second = (named[j : j + 1, :] == expert for j in range(2))
     used = jnp.where(first | second, 1.0, 0.0)
     earlier = lax.broadcasted_iota(jnp.int32, (tokens, tokens), 0)
     later = lax.broadcasted_iota(jnp.int32, (tokens, tokens), 1)
     upper = jnp.where(earlier < later, 1.0, 0.0).astype(BF16)
     rank = jnp.dot(used.astype(BF16), upper, preferred_element_type=F32)
     ranks[...] = jnp.where(first | second, rank, -1.0)
-    shares[...] = jnp.where(first, turned[2:3, :], 0.0) + jnp.where(second, turned[3:4, :], 0.0)
+    shares[...] = jnp.where(first, routes_ref[0:1, :], 0.0) + jnp.where(second, routes_ref[1:2, :], 0.0)
     slot = lax.broadcasted_iota(jnp.int32, (SLOT, tokens), 0).astype(F32)
     for g in range(GROUPS):
         weights = []
@@ -140,7 +135,6 @@
     carried,
     outbox,
     heads,
-    pairs,
     ranks,
     shares,
     select_ref,
@@ -171,6 +165,12 @@
     me = index_of(here)
     partner = (here[0], here[1], here[2], 1 - core)
     units = gate_ref.shape[1]
+    barrier = pltpu.get_barrier_semaphore()
+    others(
+        here,
+        lambda d, dev: pl.semaphore_signal(barrier, inc=1, device_id=dev, device_id_type=MESH),
+    )
+    pl.semaphore_signal(barrier, inc=1, device_id=partner, device_id_type=MESH)
     loads = {}
     for name, src, dst in (
         ("forget", forget_hbm, forget_ref),
@@ -190,12 +190,6 @@
     ):
         loads[name] = pltpu.make_async_copy(src, dst, load_sem.at[len(loads)])
         loads[name].start()
-    barrier = pltpu.get_barrier_semaphore()
-    others(
-        here,
-        lambda d, dev: pl.semaphore_signal(barrier, inc=1, device_id=dev, device_id_type=MESH),
-    )
-    pl.semaphore_signal(barrier, inc=1, device_id=partner, device_id_type=MESH)
 
     length = query_ref.shape[0]
     scale = QK ** (-0.5)
@@ -229,24 +223,6 @@
         scalars[2 + h : 3 + h, :] = jnp.broadcast_to(closing, (1, 128))
         rows_a.append(row_a)
         peaks.append(peak)
-    pl.semaphore_wait(barrier, 64)
-
-    def copy(src, dst, lane, dev):
-        return pltpu.make_async_remote_copy(
-            src_ref=src,
-            dst_ref=dst,
-            send_sem=send_sem.at[lane],
-            recv_sem=recv_sem.at[lane],
-            device_id=dev,
-            device_id_type=MESH,
-        )
-
-    def landed(ref, sem):
-        span = ref.at[pl.ds(0, 63)]
-        pltpu.make_async_copy(span, span, sem).wait()
-
-    others(here, lambda d, dev: copy(scalars, all_scalars.at[me], 0, dev).start())
-    all_scalars[me] = scalars[...]
     loads["key"].wait()
     loads["value"].wait()
     for h in range(2):
@@ -262,7 +238,28 @@
         for half in range(2):
             at = h * 32 + half * 16
             pieces[at : at + 16] = state[:, half * 128 : (half + 1) * 128].reshape(16, 8, 128)
-    others(here, lambda d, dev: copy(pieces.at[d], all_pieces.at[me], 1, dev).start())
+    pl.semaphore_wait(barrier, 64)
+
+    def copy(src, dst, lane, dev):
+        return pltpu.make_async_remote_copy(
+            src_ref=src,
+            dst_ref=dst,
+            send_sem=send_sem.at[lane],
+            recv_sem=recv_sem.at[lane],
+            device_id=dev,
+            device_id_type=MESH,
+        )
+
+    def landed(ref, sem):
+        span = ref.at[pl.ds(0, 63)]
+        pltpu.make_async_copy(span, span, sem).wait()
+
+    def spread(d, dev):
+        copy(scalars, all_scalars.at[me], 0, dev).start()
+        copy(pieces.at[d], all_pieces.at[me], 1, dev).start()
+
+    others(here, spread)
+    all_scalars[me] = scalars[...]
     all_pieces[me] = pieces[me]
 
     loads["query"].wait()
@@ -287,6 +284,7 @@
             )
             local_level[h, rows, :] = jnp.broadcast_to(level, (step, 128))
 
+    route(ids_ref, routes_ref, ranks, shares, select_ref, weigh_ref, here, loads)
     landed(all_scalars, recv_sem.at[0])
 
     def climb(s, level):
@@ -309,7 +307,6 @@
     lax.fori_loop(0, 64, scan, (jnp.zeros((8, 128), jnp.float32), jnp.zeros((1, 128), jnp.float32)))
     others(here, lambda d, dev: copy(carries.at[d], carried.at[me], 2, dev).start())
     carried[me] = carries[me]
-    route(ids_ref, routes_ref, pairs, ranks, shares, select_ref, weigh_ref, here, loads)
     landed(carried, recv_sem.at[2])
 
     span = length // 2
@@ -496,6 +493,7 @@
     half = gate_proj.shape[2]
     slots = len(OFFSETS) * SLOT
     gain = ffn_gain.reshape(1, width)
+    ids, routes = expert_ids.T, route_weights.T
     loaded = [
         stream,
         queries,
@@ -506,8 +504,8 @@
         forget_gate,
         out_proj,
         gain,
-        expert_ids,
-        route_weights,
+        ids,
+        routes,
     ]
     vmem, dma = pltpu.VMEM, pltpu.SemaphoreType.DMA
     return pl.pallas_call(
@@ -528,7 +526,6 @@
         + [
             vmem((rows_here, 2 * V_DIM), BF16),
             vmem((rows_here, 4 * V_DIM), BF16),
-            vmem((rows_here, 128), F32),
             vmem((len(OFFSETS), rows_here), F32),
             vmem((len(OFFSETS), rows_here), F32),
             vmem((slots, rows_here), BF16),
@@ -569,8 +566,8 @@
         gate_proj[0],
         up_proj[0],
         down_proj[0],
-        expert_ids,
-        route_weights,
+        ids,
+        routes,
     )
 
 

time: 150 us -> 143 us (0.953)
  Pallas kernels: 143 us -> 140 us
  local copies, waits for them, and re-layouts: 5.24 us -> 2.3 us
    pallas_call x1, Pallas kernels: 143 us -> 140 us  [body(): pl.pallas_call(layer_kernel, out_shape=jax.ShapeDtypeStruct((rows_here, w...]
    unnamed x3 -> x1, local copies, waits for them, and re-layouts: 5.24 us -> 2.3 us
where the time goes in v4:
time: 143 us; the launch traced here: 142 us
  Pallas kernels  140 us (98%)
  local copies, waits for them, and re-layouts  2.3 us (2%)
    pallas_call x1, Pallas kernels, body(): pl.pallas_call(layer_kernel, out_shape=jax.ShapeDtypeStruct((rows_here, w...  140 us

profile of v4, /device:TPU:0, one launch (start us, length us, event | category | flops | bytes accessed | tf_op | source)
XLA Modules:
  0.0 142.2 jit_solution(12507616356419192521)
XLA Ops:
  0.0 139.9 %shard_map.136 = bf16[256,2048]{1,0:T(8,128)(2,1)} custom-call(bf16[256,2048]{1,0:T(8,128)(2,1)} %stream_hbm.1, bf16[512,256]{1,0:T(8,128)(2,1)} %query_hbm.1, bf16[512,256]{1,0:T(8,128)(2,1)} %key_hbm.1, bf16[512,512]{1,0:T(8,128)(2,1)} %value_hbm.1, bf16[512,512]{1,0:T(8,128)(2,1)} %out_gate_hbm.1, f32[2,512]{1,0:T(2,128)} %in_gate_hbm.1, ...), custom_call_target="tpu_custom_call" | custom-call | tf_op jit(solution)/shard_map/pallas_call | solution.py:511
  139.9 2.3 %copy.16 = bf16[256,2048]{1,0:T(8,128)(2,1)} copy(bf16[256,2048]{1,0:T(8,128)(2,1)} %shard_map.136) | data formatting | bytes 2097152

commit v5 on v4

--- a/solution.py
+++ b/solution.py
@@ -34,15 +34,16 @@
         if orbit:
             orbits.append(orbit)
     order = [(0, 0, 0)]
-    while orbits:
-        order += orbits.pop(0)
-        if orbits:
-            order += orbits.pop()
+    for orbit in orbits:
+        order += orbit
     return order
 
 
 OFFSETS = offsets_by_orbit()
 GROUPS = len(OFFSETS) // PER_GROUP
+EARLY_GROUPS = 2
+EARLY = EARLY_GROUPS * PER_GROUP
+FIRST_WINDOW = 1
 
 
 def place():
@@ -141,6 +142,8 @@
     weigh_ref,
     middle_ref,
     normed_ref,
+    slots_out,
+    slots_in,
     outgoing,
     arrived,
     answers,
@@ -157,6 +160,8 @@
     weight_recv,
     rows_send,
     rows_recv,
+    early_recv,
+    heads_send,
     back_send,
     back_recv,
 ):
@@ -177,12 +182,12 @@
         ("in", in_gate_hbm, in_gate_ref),
         ("key", key_hbm, key_ref),
         ("value", value_hbm, value_ref),
-        ("query", query_hbm, query_ref),
         ("ids", ids_hbm, ids_ref),
         ("routes", routes_hbm, routes_ref),
+        ("stream", stream_hbm, stream_ref),
+        ("query", query_hbm, query_ref),
         ("out_gate", out_gate_hbm, out_gate_ref),
         ("out_proj", out_proj_hbm, out_proj_ref),
-        ("stream", stream_hbm, stream_ref),
         ("gain", gain_hbm, gain_ref),
         ("gate", gate_ref, gate_full.at[:, pl.ds(0, units)]),
         ("up", up_ref, up_full.at[:, pl.ds(0, units)]),
@@ -238,6 +243,46 @@
         for half in range(2):
             at = h * 32 + half * 16
             pieces[at : at + 16] = state[:, half * 128 : (half + 1) * 128].reshape(16, 8, 128)
+    route(ids_ref, routes_ref, ranks, shares, select_ref, weigh_ref, here, loads)
+    width = stream_ref.shape[1]
+    tiles = [slice(n, n + TILE) for n in range(0, width, TILE)]
+
+    def spot(i):
+        return pl.ds(i * SLOT, SLOT)
+
+    def group(g):
+        return pl.ds(g * GROUP_ROWS, GROUP_ROWS)
+
+    def members(g):
+        return range(max(g * PER_GROUP, 1), (g + 1) * PER_GROUP)
+
+    def fill(g, source, target):
+        pick = select_ref[group(g), :]
+        for n in range(0, source.shape[1], TILE):
+            cols = slice(n, n + TILE)
+            target[group(g), cols] = jnp.dot(
+                pick, source[:, cols], preferred_element_type=F32
+            ).astype(BF16)
+
+    def push(source, target, blocks, sends, lands, sign=1):
+        for i in blocks:
+            pltpu.make_async_remote_copy(
+                src_ref=source.at[spot(i)],
+                dst_ref=target.at[spot(i)],
+                send_sem=sends,
+                recv_sem=lands,
+                device_id=peer(here, OFFSETS[i], sign),
+                device_id_type=MESH,
+            ).start()
+
+    def all_in(ref, sem, first, last):
+        span = ref.at[pl.ds(first * SLOT, (last - first) * SLOT)]
+        pltpu.make_async_copy(span, span, sem).wait()
+
+    loads["stream"].wait()
+    for g in range(EARLY_GROUPS):
+        fill(g, stream_ref, outgoing)
+    arrived[spot(0), :] = outgoing[spot(0), :]
     pl.semaphore_wait(barrier, 64)
 
     def copy(src, dst, lane, dev):
@@ -259,6 +304,8 @@
         copy(pieces.at[d], all_pieces.at[me], 1, dev).start()
 
     others(here, spread)
+    for g in range(EARLY_GROUPS):
+        push(outgoing, arrived, [i for i in members(g) if i < FIRST_WINDOW], rows_send, early_recv.at[g])
     all_scalars[me] = scalars[...]
     all_pieces[me] = pieces[me]
 
@@ -284,7 +331,6 @@
             )
             local_level[h, rows, :] = jnp.broadcast_to(level, (step, 128))
 
-    route(ids_ref, routes_ref, ranks, shares, select_ref, weigh_ref, here, loads)
     landed(all_scalars, recv_sem.at[0])
 
     def climb(s, level):
@@ -306,6 +352,27 @@
 
     lax.fori_loop(0, 64, scan, (jnp.zeros((8, 128), jnp.float32), jnp.zeros((1, 128), jnp.float32)))
     others(here, lambda d, dev: copy(carries.at[d], carried.at[me], 2, dev).start())
+    weights = [
+        pltpu.make_async_remote_copy(
+            src_ref=mine_,
+            dst_ref=theirs,
+            send_sem=weight_send.at[i],
+            recv_sem=weight_recv.at[i],
+            device_id=partner,
+            device_id_type=MESH,
+        )
+        for i, (mine_, theirs) in enumerate(
+            (
+                (gate_ref, gate_full.at[:, pl.ds(units, units)]),
+                (up_ref, up_full.at[:, pl.ds(units, units)]),
+                (down_ref, down_full.at[pl.ds(units, units)]),
+            )
+        )
+    ]
+    for weight in weights:
+        weight.start()
+    for g in range(EARLY_GROUPS):
+        push(outgoing, arrived, [i for i in members(g) if i >= FIRST_WINDOW], rows_send, early_recv.at[g])
     carried[me] = carries[me]
     landed(carried, recv_sem.at[2])
 
@@ -349,32 +416,14 @@
     mine = pl.ds(pl.multiple_of(core * 2 * V_DIM, 2 * V_DIM), 2 * V_DIM)
     swap = copy(outbox, heads.at[:, mine], 3, partner)
     swap.start()
-    weights = [
-        pltpu.make_async_remote_copy(
-            src_ref=mine_,
-            dst_ref=theirs,
-            send_sem=weight_send.at[i],
-            recv_sem=weight_recv.at[i],
-            device_id=partner,
-            device_id_type=MESH,
-        )
-        for i, (mine_, theirs) in enumerate(
-            (
-                (gate_ref, gate_full.at[:, pl.ds(units, units)]),
-                (up_ref, up_full.at[:, pl.ds(units, units)]),
-                (down_ref, down_full.at[pl.ds(units, units)]),
-            )
-        )
-    ]
-    for weight in weights:
-        weight.start()
     finish(core * span, to_self)
     swap.wait()
+    for g in range(EARLY_GROUPS):
+        fill(g, heads, slots_out)
+        push(slots_out, slots_in, members(g), heads_send, rows_recv.at[g])
+    slots_in[spot(0), :] = slots_out[spot(0), :]
     loads["out_proj"].wait()
-    loads["stream"].wait()
     loads["gain"].wait()
-    width = stream_ref.shape[1]
-    tiles = [slice(n, n + TILE) for n in range(0, width, TILE)]
     squares = jnp.zeros((stream_ref.shape[0], 1), F32)
     for cols in tiles:
         mix = jnp.dot(heads[...], out_proj_ref[:, cols], preferred_element_type=F32)
@@ -386,50 +435,33 @@
     for cols in tiles:
         normed_ref[:, cols] = (middle_ref[:, cols].astype(F32) * factor * gain_ref[:, cols]).astype(BF16)
 
-    def rows(i):
-        return pl.ds(i * SLOT, SLOT)
-
-    def group(g):
-        return pl.ds(g * GROUP_ROWS, GROUP_ROWS)
-
-    def members(g):
-        return range(max(g * PER_GROUP, 1), (g + 1) * PER_GROUP)
-
-    def build(g):
-        pick = select_ref[group(g), :]
-        for cols in tiles:
-            outgoing[group(g), cols] = jnp.dot(
-                pick, normed_ref[:, cols], preferred_element_type=F32
-            ).astype(BF16)
-
-    def send(g):
-        for i in members(g):
-            pltpu.make_async_remote_copy(
-                src_ref=outgoing.at[rows(i)],
-                dst_ref=arrived.at[rows(i)],
-                send_sem=rows_send,
-                recv_sem=rows_recv.at[g],
-                device_id=peer(here, OFFSETS[i]),
-                device_id_type=MESH,
-            ).start()
-
-    build(0)
-    for g in range(1, GROUPS):
-        send(g - 1)
-        build(g)
-    arrived[rows(0), :] = outgoing[rows(0), :]
-    send(GROUPS - 1)
-
-    def all_in(ref, sem, first, last):
-        span = ref.at[pl.ds(first * SLOT, (last - first) * SLOT)]
-        pltpu.make_async_copy(span, span, sem).wait()
+    for g in range(EARLY_GROUPS, GROUPS):
+        fill(g, normed_ref, outgoing)
+        push(outgoing, arrived, members(g), rows_send, rows_recv.at[g])
 
     for name in ("gate", "up", "down"):
         loads[name].wait()
     for weight in weights:
         weight.wait_recv()
     for g in range(GROUPS):
-        all_in(arrived, rows_recv.at[g], members(g)[0], members(g)[-1] + 1)
+        if g < EARLY_GROUPS:
+            first = members(g)[0]
+            all_in(arrived, early_recv.at[g], first, (g + 1) * PER_GROUP)
+            all_in(slots_in, rows_recv.at[g], first, (g + 1) * PER_GROUP)
+            squares = jnp.zeros((GROUP_ROWS, 1), F32)
+            for cols in tiles:
+                mix = jnp.dot(slots_in[group(g), :], out_proj_ref[:, cols], preferred_element_type=F32)
+                both = (arrived[group(g), cols].astype(F32) + mix).astype(BF16)
+                arrived[group(g), cols] = both
+                both = both.astype(F32)
+                squares = squares + jnp.sum(both * both, axis=1, keepdims=True)
+            factor = lax.rsqrt(squares / width + epsilon)
+            for cols in tiles:
+                arrived[group(g), cols] = (
+                    arrived[group(g), cols].astype(F32) * factor * gain_ref[:, cols]
+                ).astype(BF16)
+        else:
+            all_in(arrived, rows_recv.at[g], members(g)[0], members(g)[-1] + 1)
         block = arrived[group(g), :]
         for n in range(0, hidden.shape[1], TILE):
             cols = slice(n, n + TILE)
@@ -440,16 +472,8 @@
             answers[group(g), cols] = jnp.dot(
                 hidden[...], down_full[:, cols], preferred_element_type=F32
             ).astype(BF16)
-        for i in members(g):
-            pltpu.make_async_remote_copy(
-                src_ref=answers.at[rows(i)],
-                dst_ref=returned.at[rows(i)],
-                send_sem=back_send,
-                recv_sem=back_recv.at[g],
-                device_id=peer(here, OFFSETS[i], -1),
-                device_id_type=MESH,
-            ).start()
-    returned[rows(0), :] = answers[rows(0), :]
+        push(answers, returned, members(g), back_send, back_recv.at[g], -1)
+    returned[spot(0), :] = answers[spot(0), :]
     for g in range(GROUPS):
         all_in(returned, back_recv.at[g], members(g)[0], members(g)[-1] + 1)
         for cols in tiles:
@@ -465,6 +489,7 @@
                 out_ref[:, cols] = (before + part).astype(out_ref.dtype)
     all_in(outgoing, rows_send, 1, len(OFFSETS))
     all_in(answers, back_send, 1, len(OFFSETS))
+    all_in(slots_out, heads_send, 1, EARLY)
     for weight in weights:
         weight.wait_send()
     for ref, lane in ((all_scalars, 0), (all_pieces, 1), (carried, 2)):
@@ -533,6 +558,7 @@
             vmem((rows_here, width), BF16),
             vmem((rows_here, width), BF16),
         ]
+        + [vmem((EARLY * SLOT, 4 * V_DIM), BF16)] * 2
         + [vmem((slots, width), BF16)] * 4
         + [
             vmem((width, 2 * half), BF16),
@@ -547,6 +573,8 @@
             dma((3,)),
             dma(()),
             dma((GROUPS,)),
+            dma((EARLY_GROUPS,)),
+            dma(()),
             dma(()),
             dma((GROUPS,)),
         ],

time: 143 us -> 132 us (0.923)
  Pallas kernels: 140 us -> 130 us
    pallas_call x1, Pallas kernels: 140 us -> 130 us  [body(): pl.pallas_call(layer_kernel, out_shape=jax.ShapeDtypeStruct((rows_here, w...]
where the time goes in v5:
time: 132 us
  Pallas kernels  130 us (98%)
  local copies, waits for them, and re-layouts  2.3 us (2%)
    pallas_call x1, Pallas kernels, body(): pl.pallas_call(layer_kernel, out_shape=jax.ShapeDtypeStruct((rows_here, w...  130 us

profile of v5, /device:TPU:0, one launch (start us, length us, event | category | flops | bytes accessed | tf_op | source)
XLA Modules:
  0.0 132.1 jit_solution(10845252982618861442)
XLA Ops:
  0.0 129.7 %shard_map.136 = bf16[256,2048]{1,0:T(8,128)(2,1)} custom-call(bf16[256,2048]{1,0:T(8,128)(2,1)} %stream_hbm.1, bf16[512,256]{1,0:T(8,128)(2,1)} %query_hbm.1, bf16[512,256]{1,0:T(8,128)(2,1)} %key_hbm.1, bf16[512,512]{1,0:T(8,128)(2,1)} %value_hbm.1, bf16[512,512]{1,0:T(8,128)(2,1)} %out_gate_hbm.1, f32[2,512]{1,0:T(2,128)} %in_gate_hbm.1, ...), custom_call_target="tpu_custom_call" | custom-call | tf_op jit(solution)/shard_map/pallas_call | solution.py:536
  129.8 2.3 %copy.16 = bf16[256,2048]{1,0:T(8,128)(2,1)} copy(bf16[256,2048]{1,0:T(8,128)(2,1)} %shard_map.136) | data formatting | bytes 2097152

commit v6 on v5

--- a/solution.py
+++ b/solution.py
@@ -43,7 +43,7 @@
 GROUPS = len(OFFSETS) // PER_GROUP
 EARLY_GROUPS = 2
 EARLY = EARLY_GROUPS * PER_GROUP
-FIRST_WINDOW = 1
+FIRST_WINDOW = 7
 
 
 def place():
@@ -128,6 +128,7 @@
     columns,
     local_num,
     local_level,
+    gates_ref,
     scalars,
     all_scalars,
     pieces,
@@ -374,6 +375,15 @@
     for g in range(EARLY_GROUPS):
         push(outgoing, arrived, [i for i in members(g) if i >= FIRST_WINDOW], rows_send, early_recv.at[g])
     carried[me] = carries[me]
+    loads["out_gate"].wait()
+    for h in range(2):
+        wide = slice(h * V_DIM, (h + 1) * V_DIM)
+        log_inter = columns[:, h : h + 1] + anchor[h : h + 1, 0:1]
+        level = local_level[h, :, 0:1]
+        peak = jnp.maximum(log_inter, level)
+        local_num[:, wide] = jnp.exp(level - peak) * local_num[:, wide]
+        local_level[h] = jnp.broadcast_to(jnp.exp(log_inter - peak), (length, 128))
+        gates_ref[:, wide] = jax.nn.sigmoid(out_gate_ref[:, wide].astype(F32))
     landed(carried, recv_sem.at[2])
 
     span = length // 2
@@ -392,17 +402,11 @@
             from_state = jnp.dot(
                 query_ref[rows, h * QK : (h + 1) * QK], state, preferred_element_type=jnp.float32
             )
-            log_inter = columns[rows, h : h + 1] + anchor[h : h + 1, 0:1]
-            level = local_level[h, rows, 0:1]
-            peak = jnp.maximum(log_inter, level)
-            number = (
-                jnp.exp(log_inter - peak) * from_state + jnp.exp(level - peak) * local_num[rows, wide]
-            )
+            number = local_level[h, rows, 0:1] * from_state + local_num[rows, wide]
             scaled = number * lax.rsqrt(
                 jnp.mean(number * number, axis=1, keepdims=True) + epsilon
             )
-            gate = jax.nn.sigmoid(out_gate_ref[rows, wide].astype(jnp.float32))
-            store(h, (scaled * gate).astype(jnp.bfloat16))
+            store(h, (scaled * gates_ref[rows, wide]).astype(jnp.bfloat16))
 
     def to_partner(h, value):
         outbox[:, h * V_DIM : (h + 1) * V_DIM] = value
@@ -411,7 +415,6 @@
         start = pl.multiple_of(core * 2 * V_DIM + h * V_DIM, V_DIM)
         heads[:, pl.ds(start, V_DIM)] = value
 
-    loads["out_gate"].wait()
     finish((1 - core) * span, to_partner)
     mine = pl.ds(pl.multiple_of(core * 2 * V_DIM, 2 * V_DIM), 2 * V_DIM)
     swap = copy(outbox, heads.at[:, mine], 3, partner)
@@ -535,7 +538,7 @@
     vmem, dma = pltpu.VMEM, pltpu.SemaphoreType.DMA
     return pl.pallas_call(
         layer_kernel,
-        out_shape=jax.ShapeDtypeStruct((rows_here, width), BF16),
+        out_shape=pltpu.VMEM((rows_here, width), BF16),
         in_specs=[pl.BlockSpec(memory_space=pl.ANY)] * 14,
         out_specs=pl.BlockSpec(memory_space=pltpu.VMEM),
         scratch_shapes=[vmem(a.shape, a.dtype) for a in loaded]
@@ -544,6 +547,7 @@
             vmem((length, 128), F32),
             vmem((length, 2 * V_DIM), F32),
             vmem((2, length, 128), F32),
+            vmem((length, 2 * V_DIM), F32),
             vmem((4, 128), F32),
             vmem((64, 4, 128), F32),
         ]

time: 132 us -> 128 us (0.970); the launches traced: 132 us -> 126 us
  Pallas kernels: 130 us -> 125 us
  local copies, waits for them, and re-layouts: 2.3 us -> 0.97 us
    pallas_call x1, Pallas kernels: 130 us -> 125 us  [body(): pl.pallas_call(layer_kernel, out_shape=pltpu.VMEM((rows_here, width), BF1...]
    unnamed x1, local copies, waits for them, and re-layouts: 2.3 us -> 0.97 us
where the time goes in v6:
time: 128 us; the launch traced here: 126 us
  Pallas kernels  125 us (98%)
    pallas_call x1, Pallas kernels, body(): pl.pallas_call(layer_kernel, out_shape=pltpu.VMEM((rows_here, width), BF1...  125 us

profile of v6, /device:TPU:0, one launch (start us, length us, event | category | flops | bytes accessed | tf_op | source)
XLA Modules:
  0.0 126.0 jit_solution(12322948001993247970)
XLA Ops:
  0.0 125.0 %shard_map.136 = bf16[256,2048]{1,0:T(8,128)(2,1)S(1)} custom-call(bf16[256,2048]{1,0:T(8,128)(2,1)} %stream_hbm.1, bf16[512,256]{1,0:T(8,128)(2,1)} %query_hbm.1, bf16[512,256]{1,0:T(8,128)(2,1)} %key_hbm.1, bf16[512,512]{1,0:T(8,128)(2,1)} %value_hbm.1, bf16[512,512]{1,0:T(8,128)(2,1)} %out_gate_hbm.1, f32[2,512]{1,0:T(2,128)} %in_gate_hbm.1, ...), custom_call_target="tpu_custom_call" | custom-call | tf_op jit(solution)/shard_map/pallas_call | solution.py:539
  125.0 1.0 copy.16

commit v7 on v6

--- a/solution.py
+++ b/solution.py
@@ -338,7 +338,6 @@
         new = jnp.maximum(all_scalars[s, 2:4, :] + level, all_scalars[s, 0:2, :])
         return jnp.where(s < me, new, level)
 
-    anchor = lax.fori_loop(0, 64, climb, jnp.zeros((2, 128), jnp.float32))
     landed(all_pieces, recv_sem.at[1])
     head = me // 32
 
@@ -351,7 +350,8 @@
         state = state * jnp.exp(moved - new) + all_pieces[s] * jnp.exp(late - new)
         return (state, new)
 
-    lax.fori_loop(0, 64, scan, (jnp.zeros((8, 128), jnp.float32), jnp.zeros((1, 128), jnp.float32)))
+    nothing = (jnp.zeros((8, 128), jnp.float32), jnp.zeros((1, 128), jnp.float32))
+    lax.fori_loop(0, 64, scan, nothing, unroll=4)
     others(here, lambda d, dev: copy(carries.at[d], carried.at[me], 2, dev).start())
     weights = [
         pltpu.make_async_remote_copy(
@@ -375,6 +375,7 @@
     for g in range(EARLY_GROUPS):
         push(outgoing, arrived, [i for i in members(g) if i >= FIRST_WINDOW], rows_send, early_recv.at[g])
     carried[me] = carries[me]
+    anchor = lax.fori_loop(0, 64, climb, jnp.zeros((2, 128), jnp.float32), unroll=4)
     loads["out_gate"].wait()
     for h in range(2):
         wide = slice(h * V_DIM, (h + 1) * V_DIM)

time: 128 us -> 136 us (1.062)
  the two profiles are of different devices: /device:TPU:0 before, /device:TPU:80 now
where the time goes in v7:
time: 136 us
  Pallas kernels  135 us (99%)
    pallas_call x1, Pallas kernels, body(): pl.pallas_call(layer_kernel, out_shape=pltpu.VMEM((rows_here, width), BF1...  135 us

profile of v7, /device:TPU:80, one launch (start us, length us, event | category | flops | bytes accessed | tf_op | source)
XLA Modules:
  0.0 136.3 jit_solution(17259579350894365358)
XLA Ops:
  0.0 135.3 %shard_map.136 = bf16[256,2048]{1,0:T(8,128)(2,1)S(1)} custom-call(bf16[256,2048]{1,0:T(8,128)(2,1)} %stream_hbm.1, bf16[512,256]{1,0:T(8,128)(2,1)} %query_hbm.1, bf16[512,256]{1,0:T(8,128)(2,1)} %key_hbm.1, bf16[512,512]{1,0:T(8,128)(2,1)} %value_hbm.1, bf16[512,512]{1,0:T(8,128)(2,1)} %out_gate_hbm.1, f32[2,512]{1,0:T(2,128)} %in_gate_hbm.1, ...), custom_call_target="tpu_custom_call" | custom-call | tf_op jit(solution)/shard_map/pallas_call | solution.py:540
  135.3 1.0 copy.16
